TPU v7x, 256 devices: a whole 4x4x8 slice. The times are simulated.
256 devices in a mesh: sp: 64 (over z, y, core), tp: 4 (over x).
Axes of the slice: x: 4, y: 4, z: 8, core: 2. Of those that a mesh axis runs over, the one named last changes fastest.
Arguments:
- head_input_values: bfloat16 [24576, 4096], P('sp', 'tp'), may hold values from -6 to 6
- group_input_vectors: bfloat16 [24576, 1024], P('sp', 'tp'), may hold values from -6 to 6
- group_readout_vectors: bfloat16 [24576, 1024], P('sp', 'tp'), may hold values from -6 to 6
- output_gate_values: bfloat16 [24576, 4096], P('sp', 'tp'), may hold values from -6 to 6
- step_size_logits: float32 [24576, 64], P('sp', 'tp'), may hold values from -6 to 6
- extra_log_decay: float32 [24576, 64], P('sp', 'tp'), may hold values from -1.2 to 0
- head_input_filter: bfloat16 [4, 4096], P(None, 'tp'), may hold values from -3 to 3
- input_vector_filter: bfloat16 [4, 1024], P(None, 'tp'), may hold values from -3 to 3
- readout_vector_filter: bfloat16 [4, 1024], P(None, 'tp'), may hold values from -3 to 3
- step_size_bias: float32 [64], P('tp'), may hold values from -0.5 to 0.5
- head_rate_logarithm: float32 [64], P('tp'), may hold values from -20 to -1
- direct_path_weight: float32 [64], P('tp'), may hold values from 0 to 3
- group_norm_scale: bfloat16 [4096], P('tp'), may hold values from 0.099609375 to 1.8984375
- mixer_output_weight: bfloat16 [4096, 2048], P('tp'), may hold values from -0.09375 to 0.09375
- residual: bfloat16 [24576, 2048], P(('sp', 'tp')), may hold values from -6 to 6
- first_norm_scale: float32 [2048], replicated, may hold values from 0.1 to 1.9
- first_norm_bias: float32 [2048], replicated, may hold values from -1.5 to 1.5
- routes: int32 [24576, 2], P(('sp', 'tp')), may hold values from 0 to 63, all different within a row; in each aligned block of 96 rows (0 to 95, 96 to 191, ...) at most 5 rows name the same one
- routing_weight: float32 [24576, 2], P(('sp', 'tp')), may hold values from 0.1 to 0.9
- expert_gate_weight: bfloat16 [64, 2048, 1024], P('sp', None, 'tp'), may hold values from -0.125 to 0.125
- expert_up_weight: bfloat16 [64, 2048, 1024], P('sp', None, 'tp'), may hold values from -0.125 to 0.125
- expert_down_weight: bfloat16 [64, 2048, 1024], P('sp', None, 'tp'), may hold values from -0.1875 to 0.1875
- final_norm_scale: float32 [2048], replicated, may hold values from 0.1 to 1.9
- final_norm_bias: float32 [2048], replicated, may hold values from -1.5 to 1.5
Outputs:
- final: bfloat16 [24576, 2048], P(('sp', 'tp'))
Inputs may be any that keep to these rules, and one draw needn't show every extreme that they name: `routes`: in the rows of one device no expert is named more than 5 times.
All inputs are finite; a program needn't handle non-finite values.
Results may differ from a plain program's by a relative error of at most 0.012.
Values may be sent and summed in bfloat16 or wider, within the bound.
No kernel may reach another device: no remote copies, remote signals or barrier semaphores. Data moves between devices by JAX's collectives and lax.ppermute only.
A program may use at most 128 MiB of HBM per device.

v0:
```python
import jax
import jax.numpy as jnp
from jax import lax
from jax.sharding import Mesh
from jax.sharding import PartitionSpec as P

HEAD_DIM = 64
STATE_WIDTH = 128
BLOCK_LENGTH = 128
SP = ("sp_0", "sp_1", "sp_2")
SP_TP = ("sp_0", "sp_1", "sp_2", "tp")


EPS = 1e-05
ALPHA = 8.0**0.25


def from_behind(block, axis, distance):
    devices = range(lax.axis_size(axis))
    route = [(i - distance, i) for i in devices if i - distance in devices]
    return lax.ppermute(block, axis, route)


def filled_with(value, identity):
    return jax.tree.map(
        lambda a, e: jnp.broadcast_to(jnp.asarray(e, a.dtype), a.shape), value, identity
    )


def prefix_by_axis(value, axes, combine, identity):
    before = start = filled_with(value, identity)
    so_far = value
    for axis in reversed(axes):
        peers, place = (lax.axis_size(axis), lax.axis_index(axis))
        pieces = jax.tree.map(
            lambda part, kind: lax.all_gather(part.astype(kind), axis),
            so_far,
            (jnp.bfloat16, jnp.bfloat16),
        )
        inside, so_far = (start, start)
        for k in range(peers):
            passed = k < place
            so_far = combine(
                so_far, jax.tree.map(lambda part, own: part[k].astype(own.dtype), pieces, value)
            )
            inside = jax.tree.map(lambda new, old: jnp.where(passed, new, old), so_far, inside)
        before = combine(inside, before)
    return before


def split_up(value, dim, peers):
    before, after = (value.shape[:dim], value.shape[dim + 1 :])
    return jnp.moveaxis(value.reshape(*before, peers, -1, *after), dim, 0)


def summed_on_arrival(value, axis, dim):
    peers = lax.axis_size(axis)
    parts = lax.all_to_all(split_up(value, dim, peers), axis, 0, 0, tiled=True)
    return jnp.sum(parts.astype(jnp.float32), axis=0)


def side_by_side(arrays, axis, dim, along):
    widths = [a.shape[along] for a in arrays]
    both = jnp.concatenate(arrays, axis=along)
    filled = lax.all_gather(both, axis, axis=dim, tiled=True)
    return tuple(jnp.split(filled, [sum(widths[:k]) for k in range(1, len(widths))], axis=along))


def layer_norm(values, gain_row, bias_row):
    mean_value = jnp.mean(values, axis=-1, keepdims=True)
    centred = values - mean_value
    spread = jnp.mean(centred * centred, axis=-1, keepdims=True)
    return centred * lax.rsqrt(spread + EPS) * gain_row + bias_row


def conv_silu(raw_rows, tail_rows, tap_weights):
    full_rows = jnp.concatenate([tail_rows, raw_rows], axis=0).astype(jnp.float32)
    weights = tap_weights.astype(jnp.float32)
    length = raw_rows.shape[0]
    summed_output = jnp.zeros((length, raw_rows.shape[1]), jnp.float32)
    for offset in range(tap_weights.shape[0]):
        summed_output = summed_output + weights[offset] * full_rows[offset : offset + length]
    return jax.nn.silu(summed_output)


def block_pass(state_now, input_blocks):
    step_scaled_inputs, decay_logarithm, inputs_b, reads_c = input_blocks
    running = jnp.cumsum(decay_logarithm, axis=0)
    running_t = jnp.moveaxis(running, 0, -1)
    length = decay_logarithm.shape[0]
    causal = jnp.arange(length)[:, None] >= jnp.arange(length)[None, :]
    spread_log = jnp.where(causal, running_t[..., :, None] - running_t[..., None, :], -jnp.inf)
    decay_factors = jnp.exp(spread_log)
    decay_products = jnp.einsum("tgn,sgn->gts", reads_c, inputs_b)
    within_block_output = jnp.einsum(
        "zmka,azmo->kzmo", decay_products[:, None] * decay_factors, step_scaled_inputs
    )
    carried_in = jnp.einsum("tgn,grpn->tgrp", reads_c, state_now) * jnp.exp(running)[..., None]
    to_end = jnp.exp(running_t[..., -1:] - running_t)
    added = jnp.einsum("sgn,grs,sgrp->grpn", inputs_b, to_end, step_scaled_inputs)
    state_next = jnp.exp(running_t[..., -1])[..., None, None] * state_now + added
    return (state_next, within_block_output + carried_in)


def chain_states(earlier, later):
    return (earlier[0] + later[0], jnp.exp(later[0])[..., None, None] * earlier[1] + later[1])


def slot_layout(block_routes, capacity, experts):
    flat_routes = block_routes.reshape(-1)
    matches = (flat_routes[:, None] == jnp.arange(experts, dtype=jnp.int32)[None, :]).astype(
        jnp.int32
    )
    before = jnp.cumsum(matches, axis=0) - matches
    return flat_routes * capacity + jnp.sum(before * matches, axis=1)


def expert_hidden(arrived, weight_gate, weight_up):
    local_count = weight_gate.shape[0]
    grouped = arrived.reshape(-1, local_count, arrived.shape[1], arrived.shape[2])
    gate_part = jnp.einsum(
        "send,edf->senf", grouped, weight_gate, preferred_element_type=jnp.float32
    )
    up_part = jnp.einsum("send,edf->senf", grouped, weight_up, preferred_element_type=jnp.float32)
    return (jax.nn.silu(gate_part) * up_part).astype(jnp.bfloat16)


def expert_output(hidden, weight_down):
    result = jnp.einsum("senf,edf->send", hidden, weight_down, preferred_element_type=jnp.float32)
    return result.reshape(-1, result.shape[2], result.shape[3])


def shards(
    head_input_values,
    group_input_vectors,
    group_readout_vectors,
    output_gate_values,
    step_size_logits,
    extra_log_decay,
    head_input_filter,
    input_vector_filter,
    readout_vector_filter,
    step_size_bias,
    head_rate_logarithm,
    direct_path_weight,
    group_norm_scale,
    mixer_output_weight,
    residual,
    first_norm_scale,
    first_norm_bias,
    routes,
    routing_weight,
    expert_gate_weight,
    expert_up_weight,
    expert_down_weight,
    final_norm_scale,
    final_norm_bias,
):
    length = head_input_values.shape[0]
    margin = head_input_filter.shape[0] - 1
    tail_x, tail_b, tail_c = from_behind(
        (
            head_input_values[length - margin :],
            group_input_vectors[length - margin :],
            group_readout_vectors[length - margin :],
        ),
        SP,
        1,
    )
    conv_x = conv_silu(head_input_values, tail_x, head_input_filter)
    conv_b = conv_silu(group_input_vectors, tail_b, input_vector_filter)
    conv_c = conv_silu(group_readout_vectors, tail_c, readout_vector_filter)
    heads_here = head_input_values.shape[1] // HEAD_DIM
    groups_here = group_input_vectors.shape[1] // STATE_WIDTH
    repeat_count = heads_here // groups_here
    step_sizes = jax.nn.softplus(step_size_logits + step_size_bias)
    decay_logarithm = -step_sizes * jnp.exp(head_rate_logarithm) + extra_log_decay
    heads_x = conv_x.reshape(length, groups_here, repeat_count, HEAD_DIM)
    step_scaled_inputs = heads_x * step_sizes.reshape(length, groups_here, repeat_count)[..., None]
    decay_heads = decay_logarithm.reshape(length, groups_here, repeat_count)
    inputs_b = conv_b.reshape(length, groups_here, STATE_WIDTH)
    reads_c = conv_c.reshape(length, groups_here, STATE_WIDTH)
    block_list = length // BLOCK_LENGTH
    start_state = jnp.zeros((groups_here, repeat_count, HEAD_DIM, STATE_WIDTH), jnp.float32)
    end_state, within_block_output = lax.scan(
        block_pass,
        start_state,
        (
            step_scaled_inputs.reshape(
                block_list, BLOCK_LENGTH, groups_here, repeat_count, HEAD_DIM
            ),
            decay_heads.reshape(block_list, BLOCK_LENGTH, groups_here, repeat_count),
            inputs_b.reshape(block_list, BLOCK_LENGTH, groups_here, STATE_WIDTH),
            reads_c.reshape(block_list, BLOCK_LENGTH, groups_here, STATE_WIDTH),
        ),
    )
    total_decay = jnp.sum(decay_heads, axis=0)
    identity = (jnp.zeros_like(total_decay), jnp.zeros_like(end_state))
    earlier_part = prefix_by_axis((total_decay, end_state), SP, chain_states, identity)
    incoming = earlier_part[1]
    device_running = jnp.cumsum(decay_heads, axis=0)
    readout = jnp.einsum("tgn,grpn->tgrp", reads_c, incoming) * jnp.exp(device_running)[..., None]
    ssm_out = (
        within_block_output.reshape(length, groups_here, repeat_count, HEAD_DIM)
        + readout
        + direct_path_weight.reshape(groups_here, repeat_count)[None, :, :, None] * heads_x
    )
    gated = ssm_out.reshape(length, -1) * jax.nn.silu(output_gate_values.astype(jnp.float32))
    grouped = gated.reshape(length, groups_here, -1)
    normed = grouped * lax.rsqrt(jnp.mean(grouped * grouped, axis=-1, keepdims=True) + EPS)
    mixer_rows = (normed.reshape(length, -1) * group_norm_scale.astype(jnp.float32)).astype(
        jnp.bfloat16
    )
    rows_here = residual.shape[0]
    mixed = summed_on_arrival(
        jnp.dot(mixer_rows, mixer_output_weight, preferred_element_type=jnp.float32).astype(
            jnp.bfloat16
        ),
        "tp",
        0,
    )
    middle = layer_norm(
        ALPHA * residual.astype(jnp.float32) + mixed, first_norm_scale, first_norm_bias
    ).astype(jnp.bfloat16)
    top_count = routes.shape[1]
    width = middle.shape[1]
    experts = expert_gate_weight.shape[0] * lax.axis_size(SP)
    capacity = max(2, rows_here * top_count * 5 // (3 * experts))
    slot_ids = slot_layout(routes, capacity, experts)
    owners = jnp.repeat(jnp.arange(rows_here, dtype=jnp.int32), top_count)
    source = jnp.full((experts * capacity,), rows_here, jnp.int32).at[slot_ids].set(owners)
    padded = jnp.concatenate([middle, jnp.zeros((1, width), jnp.bfloat16)], axis=0)
    outgoing = padded[source].reshape(experts, capacity, width)
    whole_gate, whole_up, whole_down = side_by_side(
        (expert_gate_weight, expert_up_weight, expert_down_weight), "tp", 2, 0
    )
    hidden = expert_hidden(
        lax.all_to_all(outgoing, SP, split_axis=0, concat_axis=0, tiled=True), whole_gate, whole_up
    )
    answers = expert_output(hidden, whole_down).astype(jnp.bfloat16)
    returned = lax.all_to_all(answers, SP, split_axis=0, concat_axis=0, tiled=True)
    picked = (
        returned.reshape(-1, width)[slot_ids]
        .astype(jnp.float32)
        .reshape(rows_here, top_count, width)
    )
    ffn = jnp.sum(picked * routing_weight[..., None], axis=1)
    return layer_norm(
        ALPHA * middle.astype(jnp.float32) + ffn, final_norm_scale, final_norm_bias
    ).astype(jnp.bfloat16)


def solution(mesh):
    split = Mesh(mesh.devices.reshape(8, 4, 2, mesh.shape["tp"]), ("sp_0", "sp_1", "sp_2", "tp"))
    placed = (
        P(SP, "tp"),
        P(SP, "tp"),
        P(SP, "tp"),
        P(SP, "tp"),
        P(SP, "tp"),
        P(SP, "tp"),
        P(None, "tp"),
        P(None, "tp"),
        P(None, "tp"),
        P("tp"),
        P("tp"),
        P("tp"),
        P("tp"),
        P("tp", None),
        P(SP_TP, None),
        P(),
        P(),
        P(SP_TP, None),
        P(SP_TP, None),
        P(SP, None, "tp"),
        P(SP, None, "tp"),
        P(SP, None, "tp"),
        P(),
        P(),
    )
    return jax.shard_map(
        shards, mesh=split, in_specs=placed, out_specs=P(SP_TP, None), check_vma=False
    )
```

profile of v0, /device:TPU:8, one launch (start us, length us, event | category | flops | bytes accessed | tf_op | source)
XLA Modules:
  0.0 397.1 jit_solution(11025642554368086106)
XLA Ops:
  9.9 3.6 collective-permute-start.2
  20.4 2.8 all_gather.29
  32.7 53.9 %while.13 = (s32[]{:T(128)}, f32[2,8,64,128]{3,2,1,0:T(8,128)S(1)}, f32[3,128,2,8,64]{1,0,4,3,2:T(4,128)}, f32[3,128,2,8]{1,0,3,2:T(4,128)S(1)}, f32[3,128,2,8,6...) while((s32[]{:T(128)}, f32[2,8,64,128]{3,2,1,0:T(8,128)S(1)}, ...), condition=%wide.region_2.3_spmd.clone, body=%wide.region_0.2_spmd.clone.sunk | while | flops 111034368 | bytes 7258616 | solution.py:185
  36.4 13.8 %dynamic_update_slice.6 = f32[3,128,2,8,64]{1,0,4,3,2:T(4,128)} dynamic-update-slice(f32[3,128,2,8,64]{1,0,4,3,2:T(4,128)} %get-tuple-element.209, f32[1,128,2,8,64]{1,0,4,3,2:T(1,128)S(1)} %bitcast.346, s32[]{:T(128)} %get-tuple-element.207, s32[]{:T(128)} %constant.42.clone.1..sunk, s32[]{:T(128)} %constant.42.clone.1..sunk, s32[]{:T(128)} %constant.42.clone.1..sunk, s32[]{:T(128)} %constant.42.clone.1..sunk) | dynamic-update-slice | bytes 1048580 | tf_op jit(solution)/shard_map/while/body/jit(dynamic_update_index_in_dim)/dynamic_update_slice | solution.py:185
  54.4 13.8 %dynamic_update_slice.6 = f32[3,128,2,8,64]{1,0,4,3,2:T(4,128)} dynamic-update-slice(f32[3,128,2,8,64]{1,0,4,3,2:T(4,128)} %get-tuple-element.209, f32[1,128,2,8,64]{1,0,4,3,2:T(1,128)S(1)} %bitcast.346, s32[]{:T(128)} %get-tuple-element.207, s32[]{:T(128)} %constant.42.clone.1..sunk, s32[]{:T(128)} %constant.42.clone.1..sunk, s32[]{:T(128)} %constant.42.clone.1..sunk, s32[]{:T(128)} %constant.42.clone.1..sunk) | dynamic-update-slice | bytes 1048580 | tf_op jit(solution)/shard_map/while/body/jit(dynamic_update_index_in_dim)/dynamic_update_slice | solution.py:185
  72.4 13.8 %dynamic_update_slice.6 = f32[3,128,2,8,64]{1,0,4,3,2:T(4,128)} dynamic-update-slice(f32[3,128,2,8,64]{1,0,4,3,2:T(4,128)} %get-tuple-element.209, f32[1,128,2,8,64]{1,0,4,3,2:T(1,128)S(1)} %bitcast.346, s32[]{:T(128)} %get-tuple-element.207, s32[]{:T(128)} %constant.42.clone.1..sunk, s32[]{:T(128)} %constant.42.clone.1..sunk, s32[]{:T(128)} %constant.42.clone.1..sunk, s32[]{:T(128)} %constant.42.clone.1..sunk) | dynamic-update-slice | bytes 1048580 | tf_op jit(solution)/shard_map/while/body/jit(dynamic_update_index_in_dim)/dynamic_update_slice | solution.py:185
  90.0 7.9 %all_gather.30 = bf16[4,2,8]{2,1,0:T(2,128)(2,1)S(1)} all-gather(bf16[1,2,8]{2,1,0:T(2,128)(2,1)S(1)} %get-tuple-element.145), channel_id=1, replica_groups=mesh['sp_0'=8,'sp_1'=4,'sp_2'=2,'tp'=4] {'sp_1'}, dimensions={0}, use_global_device_ids=true | all-gather | bytes 160 | tf_op jit(solution)/shard_map/all_gather | solution.py:36
  98.0 19.7 %all-gather.5.cloned.1.call-done = bf16[4,2,8,64,128]{4,3,2,1,0:T(8,128)(2,1)} async-done(((bf16[1,2,8,64,128]{4,3,2,1,0:T(8,128)(2,1)}), bf16[4,2,8,64,128]{4,3,2,1,0:T(8,128)(2,1)}) %all-gather.5.cloned.1.call-update) | async-done | bytes 1048592 | tf_op jit(solution)/shard_map/all_gather | solution.py:36
  120.1 3.6 pad_maximum_fusion
  126.6 16.8 %all_gather.31 = bf16[8,2,8]{2,1,0:T(2,128)(2,1)S(1)} all-gather(bf16[1,2,8]{2,1,0:T(2,128)(2,1)S(1)} %get-tuple-element.132), channel_id=1, replica_groups=mesh['sp_0'=8,'sp_1'=4,'sp_2'=2,'tp'=4] {'sp_0'}, dimensions={0}, use_global_device_ids=true | all-gather | bytes 288 | tf_op jit(solution)/shard_map/all_gather | solution.py:36
  143.5 3.9 reshape.383
  147.4 15.1 %all-gather.7.cloned.1.call-done = bf16[8,2,8,64,128]{4,3,2,1,0:T(8,128)(2,1)} async-done(((bf16[1,2,8,64,128]{4,3,2,1,0:T(8,128)(2,1)}), bf16[8,2,8,64,128]{4,3,2,1,0:T(8,128)(2,1)}) %all-gather.7.cloned.1.call-update) | async-done | bytes 2097168 | tf_op jit(solution)/shard_map/all_gather | solution.py:36
  162.5 4.9 %fusion.43 = f32[384,2,8,64]{0,3,2,1:T(8,128)} fusion(f32[384,2,8,64]{0,3,2,1:T(8,128)} %reshape.383, f32[384,2,8,64]{0,3,2,1:T(8,128)S(1)} %bitcast.350, f32[2,8]{1,0:T(2,128)S(1)} %mul.557, f32[384,2,8]{0,2,1:T(8,128)S(1)} %bitcast_bitcast_fusion.1, bf16[384,2,128,1]{2,1,0,3:T(2,128)(2,1)S(1)} %bitcast.354, ...), kind=kOutput, calls=%fused_computation.69 | convolution fusion | flops 109707264 | bytes 8610894 | tf_op jit(solution)/shard_map/tgn,grpn->tgrp/dot_general | solution.py:202
  177.3 3.2 convolution_convert_fusion
  180.5 4.3 %all-to-all-start = ((bf16[4,96,2048]{2,1,0:T(8,128)(2,1)}), bf16[4,96,2048]{2,1,0:T(8,128)(2,1)S(1)}, u32[]{:S(2)}, u32[]{:S(2)}) async-start(bf16[4,96,2048]{2,1,0:T(8,128)(2,1)} %bitcast.50), calls=%async_computation | async-start | bytes 3145728 | tf_op jit(solution)/shard_map/all_to_all | solution.py:58
  186.7 34.9 %all-to-all-done = bf16[4,96,2048]{2,1,0:T(8,128)(2,1)S(1)} async-done(((bf16[4,96,2048]{2,1,0:T(8,128)(2,1)}), bf16[4,96,2048]{2,1,0:T(8,128)(2,1)S(1)}, u32[]{:S(2)}, u32[]{:S(2)}) %all-to-all-start) | async-done | bytes 1572896 | tf_op jit(solution)/shard_map/all_to_all | solution.py:58
  222.9 3.0 gather_fusion
  228.3 58.6 %all_to_all.15 = bf16[64,5,2048]{2,1,0:T(8,128)(2,1)} all-to-all(bf16[64,5,2048]{2,1,0:T(8,128)(2,1)S(1)} %reshape.396), channel_id=1, replica_groups=mesh['sp_0'=8,'sp_1'=4,'sp_2'=2,'tp'=4] {'sp_0','sp_1','sp_2'}, dimensions={0} | all-to-all | bytes 2621440 | tf_op jit(solution)/shard_map/all_to_all | solution.py:238
  286.9 17.9 %all-gather.9.cloned.1.call-done = bf16[3,2048,1024]{2,1,0:T(8,128)(2,1)} async-done(((bf16[3,2048,256]{2,1,0:T(8,128)(2,1)}), bf16[3,2048,1024]{2,1,0:T(8,128)(2,1)}) %all-gather.9.cloned.1.call-update) | async-done | bytes 12582928 | tf_op jit(solution)/shard_map/all_gather | solution.py:65
  304.9 5.8 %fusion.44 = f32[64,1,5,1024]{3,0,2,1:T(8,128)} fusion(bf16[3,2048,1024]{2,1,0:T(8,128)(2,1)} %all-gather.9.cloned.1.call-done, bf16[64,5,2048]{2,1,0:T(8,128)(2,1)} %all_to_all.15), kind=kOutput, calls=%fused_computation.73 | convolution fusion | flops 1342177280 | bytes 7602176 | tf_op jit(solution)/shard_map/send,edf->senf/dot_general | solution.py:121
  310.6 8.1 %fusion.34 = bf16[64,5,2048]{2,0,1:T(8,128)(2,1)} fusion(bf16[3,2048,1024]{2,1,0:T(8,128)(2,1)} %all-gather.9.cloned.1.call-done, f32[64,1,5,1024]{3,0,2,1:T(8,128)} %fusion.44, bf16[64,5,2048]{2,1,0:T(8,128)(2,1)S(1)} %copy-done.2), kind=kOutput, calls=%fused_computation.53 | convolution fusion | flops 2686976000 | bytes 12320768 | tf_op jit(solution)/shard_map/senf,edf->send/dot_general | solution.py:129
  318.8 3.4 copy.132
  322.2 8.5 %all-to-all-start.2 = ((bf16[64,5,2048]{2,1,0:T(8,128)(2,1)}), bf16[64,5,2048]{2,1,0:T(8,128)(2,1)}, u32[]{:S(2)}, u32[]{:S(2)}) async-start(bf16[64,5,2048]{2,1,0:T(8,128)(2,1)} %copy.132), calls=%async_computation.2 | async-start | bytes 4194304 | tf_op jit(solution)/shard_map/all_to_all | solution.py:241
  330.9 51.0 %all-to-all-done.2 = bf16[64,5,2048]{2,1,0:T(8,128)(2,1)} async-done(((bf16[64,5,2048]{2,1,0:T(8,128)(2,1)}), bf16[64,5,2048]{2,1,0:T(8,128)(2,1)}, u32[]{:S(2)}, u32[]{:S(2)}) %all-to-all-start.2) | async-done | bytes 1310752 | tf_op jit(solution)/shard_map/all_to_all | solution.py:241
  (179 shorter events, 64.5 us)
Async XLA Ops:
  6.5 18.0 %copy-start.7 = (bf16[384,256]{1,0:T(8,128)(2,1)S(1)}, bf16[384,256]{1,0:T(8,128)(2,1)}, u32[]{:S(2)}) copy-start(bf16[384,256]{1,0:T(8,128)(2,1)} %param.27) | copy-start | bytes 589828
  6.5 111.2 %all-gather.5.cloned.1.call-start = ((), (), s32[]{:S(2)}) async-start(), calls=%async_computation.3 | async-start | bytes 1310720 | tf_op jit(solution)/shard_map/all_gather | solution.py:36
  7.3 17.7 %collective-permute-start = (bf16[3,1024]{1,0:T(4,128)(2,1)S(1)}, bf16[3,1024]{1,0:T(4,128)(2,1)S(1)}, u32[]{:S(2)}, u32[]{:S(2)}) collective-permute-start(bf16[3,1024]{1,0:T(4,128)(2,1)S(1)} %slice.185), channel_id=1, source_target_pairs={{0,4},{4,8},{8,12},{12,16},{16,20},{20,24},{24,28},{28,32},{32,36}... | collective-permute-start | bytes 18440 | tf_op jit(solution)/shard_map/ppermute | solution.py:21
  9.9 13.4 %collective-permute-start.2 = (bf16[3,256]{1,0:T(4,128)(2,1)S(1)}, bf16[3,256]{1,0:T(4,128)(2,1)S(1)}, u32[]{:S(2)}, u32[]{:S(2)}) collective-permute-start(bf16[3,256]{1,0:T(4,128)(2,1)S(1)} %slice.203), channel_id=1, source_target_pairs={{0,4},{4,8},{8,12},{12,16},{16,20},{20,24},{24,28},{28,32},{32,36}... | collective-permute-start | bytes 4616 | tf_op jit(solution)/shard_map/ppermute | solution.py:21
  14.2 10.3 %collective-permute-start.1 = (bf16[3,256]{1,0:T(4,128)(2,1)S(1)}, bf16[3,256]{1,0:T(4,128)(2,1)S(1)}, u32[]{:S(2)}, u32[]{:S(2)}) collective-permute-start(bf16[3,256]{1,0:T(4,128)(2,1)S(1)} %slice.194), channel_id=1, source_target_pairs={{0,4},{4,8},{8,12},{12,16},{16,20},{20,24},{24,28},{28,32},{32,36}... | collective-permute-start | bytes 4616 | tf_op jit(solution)/shard_map/ppermute | solution.py:21
  24.5 1.1 copy-start.4
  86.7 33.4 %copy-start.3 = (bf16[1,2048,256]{2,1,0:T(8,128)(2,1)S(1)}, bf16[1,2048,256]{2,1,0:T(8,128)(2,1)}, u32[]{:S(2)}) copy-start(bf16[1,2048,256]{2,1,0:T(8,128)(2,1)} %param.47) | copy-start | bytes 3145732
  90.0 72.5 %all-gather.7.cloned.1.call-start = ((), (), s32[]{:S(2)}) async-start(), calls=%async_computation.4 | async-start | bytes 2359296 | tf_op jit(solution)/shard_map/all_gather | solution.py:36
  120.0 184.9 %all-gather.9.cloned.1.call-start = ((), (), s32[]{:S(2)}) async-start(), calls=%async_computation.5 | async-start | bytes 15728640 | tf_op jit(solution)/shard_map/all_gather | solution.py:65
  123.6 2.0 copy-start.16
  123.6 2.0 copy-start.13
  123.6 2.0 copy-start.12
  143.5 19.0 %copy-start = (f32[384,1024]{0,1:T(8,128)S(1)}, f32[384,1024]{0,1:T(8,128)}, u32[]{:S(2)}) copy-start(f32[384,1024]{0,1:T(8,128)} %copy.112) | copy-start | bytes 4718596
  167.4 2.0 copy-start.5
  174.1 2.8 copy-start.15
  174.7 2.6 copy-start.6
  180.5 41.2 %all-to-all-start = ((bf16[4,96,2048]{2,1,0:T(8,128)(2,1)}), bf16[4,96,2048]{2,1,0:T(8,128)(2,1)S(1)}, u32[]{:S(2)}, u32[]{:S(2)}) async-start(bf16[4,96,2048]{2,1,0:T(8,128)(2,1)} %bitcast.50), calls=%async_computation | async-start | bytes 3145728 | tf_op jit(solution)/shard_map/all_to_all | solution.py:58
  184.7 37.2 %copy-start.1 = (bf16[96,2048]{1,0:T(8,128)(2,1)S(1)}, bf16[96,2048]{1,0:T(8,128)(2,1)}, u32[]{:S(2)}) copy-start(bf16[96,2048]{1,0:T(8,128)(2,1)} %param.40) | copy-start | bytes 1179652
  221.9 0.7 copy-start.8
  222.0 0.7 copy-start.9
  286.9 23.7 %copy-start.2 = (bf16[64,5,2048]{2,1,0:T(8,128)(2,1)S(1)}, bf16[64,5,2048]{2,1,0:T(8,128)(2,1)}, u32[]{:S(2)}) copy-start(bf16[64,5,2048]{2,1,0:T(8,128)(2,1)} %all_to_all.15) | copy-start | bytes 3932164
  322.2 8.6 %copy-start.14 = (f32[96,2]{0,1:T(2,128)S(1)}, f32[96,2]{0,1:T(2,128)}, u32[]{:S(2)}) copy-start(f32[96,2]{0,1:T(2,128)} %param.44) | copy-start | bytes 2308
  322.2 59.7 %all-to-all-start.2 = ((bf16[64,5,2048]{2,1,0:T(8,128)(2,1)}), bf16[64,5,2048]{2,1,0:T(8,128)(2,1)}, u32[]{:S(2)}, u32[]{:S(2)}) async-start(bf16[64,5,2048]{2,1,0:T(8,128)(2,1)} %copy.132), calls=%async_computation.2 | async-start | bytes 4194304 | tf_op jit(solution)/shard_map/all_to_all | solution.py:241
  388.9 0.7 copy-start.11
  (1 other events, 0.7 us)
Sparse Core Ops, SparseCore 0:
  90.1 27.5 all-gather.4
  120.1 42.3 all-gather.6
  164.3 140.5 all-gather.8
where the time goes:
time: 399 us; the launch traced here: 397 us
  waiting for transfers between devices  139 us (35%)
  blocking collectives  88.5 us (22%)
  local copies, waits for them, and re-layouts  87.6 us (22%)
  matrix products  25.7 us (6%)
  other arithmetic  22.4 us (6%)
  starting transfers between devices  20.3 us (5%)
  between operations  13.6 us (3%)
    all_to_all x1, blocking collectives, shards(): lax.all_to_all(outgoing, SP, split_axis=0, concat_axis=0, tiled=True)  58.6 us
    all_to_all x1, waiting for transfers between devices, shards(): lax.all_to_all(answers, SP, split_axis=0, concat_axis=0, tiled=True)  51 us
    dynamic_update_slice x3, local copies, waits for them, and re-layouts, shards(): lax.scan(block_pass, start_state, (step_scaled_inputs.reshape(block_list,...  41.5 us
    all_to_all x1, waiting for transfers between devices, summed_on_arrival(): parts = lax.all_to_all(split_up(value, dim, peers), axis, 0, 0, tiled=True)  34.9 us
    all_gather x2, waiting for transfers between devices, prefix_by_axis(): lax.all_gather(part.astype(kind), axis)  34.8 us
    all_gather x4, blocking collectives, prefix_by_axis(): lax.all_gather(part.astype(kind), axis)  29.9 us
    all_gather x1, waiting for transfers between devices, side_by_side(): filled = lax.all_gather(both, axis, axis=dim, tiled=True)  17.9 us
    all_to_all x1, starting transfers between devices, shards(): lax.all_to_all(answers, SP, split_axis=0, concat_axis=0, tiled=True)  8.55 us
  transfers between devices with their start and end apart: 8, of which 5 were waited for; matrix products, arithmetic and copies ran while one was open for 11% of the time, Pallas kernels for 0%

commit v1 on v0

v1 whole, which is shorter than its diff:
```python
import jax
import jax.numpy as jnp
from jax import lax
from jax.experimental import pallas as pl
from jax.experimental.pallas import tpu as pltpu
from jax.sharding import PartitionSpec as P


HEAD_DIM = 64
STATE_WIDTH = 128
BLOCK = 128
LANES = 128
SP = "sp"
SP_TP = ("sp", "tp")
EPS = 1e-05
ALPHA = 8.0**0.25
F32 = jnp.float32
BF16 = jnp.bfloat16

VMEM = pl.BlockSpec(memory_space=pltpu.VMEM)
SMEM = pl.BlockSpec(memory_space=pltpu.SMEM)
ANY = pl.BlockSpec(memory_space=pl.ANY)


def limit(mib):
    return pltpu.CompilerParams(vmem_limit_bytes=mib * 1024 * 1024)


def shape_of(shape, dtype):
    return jax.ShapeDtypeStruct(shape, dtype)


def near(shape, dtype):
    return pltpu.VMEM(shape, dtype)


def held(value):
    return pltpu.with_memory_space_constraint(value, pltpu.VMEM)


def far_off(*values):
    return [pltpu.with_memory_space_constraint(value, pltpu.HBM) for value in values]


def dot(a, b, dims=((1,), (0,))):
    return lax.dot_general(a, b, (dims, ((), ())), preferred_element_type=F32)


def silu(v):
    return v * (1.0 / (1.0 + jnp.exp(-v)))


def spread_heads(values, group, heads, width):
    total = values.shape[1]
    row = lax.broadcasted_iota(jnp.int32, (total, width), 0)
    col = lax.broadcasted_iota(jnp.int32, (total, width), 1)
    first = group * heads + col // HEAD_DIM
    pick = jnp.where(row == first, 1.0, 0.0).astype(BF16)
    high = values.astype(BF16)
    low = (values - high.astype(F32)).astype(BF16)
    return dot(high, pick) + dot(low, pick)


def fill_rows(rows_ref, tail_ref, raw_ref, cols, offset, length):
    rows_ref[0:8, :] = tail_ref[:, offset + cols.start : offset + cols.stop].astype(F32)
    rows_ref[8 : 8 + length, :] = raw_ref[:, cols].astype(F32)


def conv_cols(rows_ref, taps, length, margin):
    total = taps[0:1, :] * rows_ref[8 - margin : 8 - margin + length, :]
    for k in range(1, margin + 1):
        total = total + taps[k : k + 1, :] * rows_ref[8 - margin + k : 8 - margin + k + length, :]
    return silu(total)


def turned(ref):
    rows, length = ref.shape
    parts = []
    for i in range(0, length, BLOCK):
        tall = jnp.concatenate([ref[:, i : i + BLOCK], jnp.zeros((BLOCK - rows, BLOCK), F32)], axis=0)
        parts.append(tall.T[:, :rows])
    return jnp.concatenate(parts, axis=0)


def log_decays(logits_ref, extra_ref, bias_ref, rate_ref):
    raw = turned(logits_ref) + bias_ref[...]
    step = jnp.maximum(raw, 0.0) + jnp.log1p(jnp.exp(-jnp.abs(raw)))
    return step, -step * jnp.exp(rate_ref[...]) + turned(extra_ref)


def running_sum(block):
    t = lax.broadcasted_iota(jnp.int32, (BLOCK, BLOCK), 0)
    s = lax.broadcasted_iota(jnp.int32, (BLOCK, BLOCK), 1)
    lower = jnp.where(t >= s, 1.0, 0.0)
    return jnp.dot(lower, block, precision=lax.Precision.HIGHEST, preferred_element_type=F32)


def end_state_kernel(
    x_ref,
    b_ref,
    tail_ref,
    xf_ref,
    bf_ref,
    logits_ref,
    extra_ref,
    bias_ref,
    rate_ref,
    xc_ref,
    xdt_ref,
    bc_ref,
    running_ref,
    states_ref,
    message_ref,
    rows_ref,
):
    length, channels = x_ref.shape
    margin = xf_ref.shape[0] - 1
    groups = b_ref.shape[1] // STATE_WIDTH
    width = channels // groups
    heads = width // HEAD_DIM
    blocks = length // BLOCK
    step, decay = log_decays(logits_ref, extra_ref, bias_ref, rate_ref)
    sums = []
    for i in range(blocks):
        part = running_sum(decay[i * BLOCK : (i + 1) * BLOCK])
        running_ref[i * BLOCK : (i + 1) * BLOCK, :] = part
        sums.append(part)
    for c in range(0, groups * STATE_WIDTH, LANES):
        cols = slice(c, c + LANES)
        fill_rows(rows_ref, tail_ref, b_ref, cols, channels, length)
        bc_ref[:, cols] = conv_cols(rows_ref, bf_ref[:, cols].astype(F32), length, margin).astype(BF16)
    for c in range(0, channels, LANES):
        cols = slice(c, c + LANES)
        fill_rows(rows_ref, tail_ref, x_ref, cols, 0, length)
        xc_ref[:, cols] = conv_cols(rows_ref, xf_ref[:, cols].astype(F32), length, margin).astype(BF16)
    total = jnp.zeros((1, decay.shape[1]), F32)
    for i in range(blocks):
        total = total + sums[i][BLOCK - 1 : BLOCK]
    tiles = width // LANES
    for g in range(groups):
        state = None
        for i in range(blocks):
            rows = slice(i * BLOCK, (i + 1) * BLOCK)
            here = slice(g * width, (g + 1) * width)
            ending = sums[i][BLOCK - 1 : BLOCK]
            step_wide = spread_heads(step[rows], g, heads, width)
            left_wide = spread_heads(jnp.exp(ending - sums[i]), g, heads, width)
            scaled = xc_ref[rows, here].astype(F32) * step_wide
            xdt_ref[rows, here] = scaled.astype(BF16)
            keys = bc_ref[rows, g * STATE_WIDTH : (g + 1) * STATE_WIDTH].astype(F32).T.astype(BF16)
            added = dot(keys, (scaled * left_wide).astype(BF16))
            if state is None:
                state = added
            else:
                state = state * spread_heads(jnp.exp(ending), g, heads, width) + added
            if i + 1 < blocks:
                states_ref[i, g] = state
        high = total.astype(BF16)
        rest = total - high.astype(F32)
        low = rest.astype(BF16)
        least = (rest - low.astype(F32)).astype(BF16)
        parts = jnp.concatenate([high, low, least, jnp.zeros((5, total.shape[1]), BF16)], axis=0)
        logs = spread_heads(parts.astype(F32), g, heads, width).astype(BF16)
        for n in range(STATE_WIDTH // 16):
            for p in range(tiles):
                at = (g * (STATE_WIDTH // 16) + n) * tiles + p
                message_ref[at, 0:16, :] = state[n * 16 : (n + 1) * 16, p * LANES : (p + 1) * LANES].astype(BF16)
                message_ref[at, 16:24, :] = logs[:, p * LANES : (p + 1) * LANES]


def end_states(x, b, tail, xf, bf, logits, extra, bias, rate):
    length, channels = x.shape
    groups = b.shape[1] // STATE_WIDTH
    blocks = length // BLOCK
    width = channels // groups
    pieces = groups * STATE_WIDTH * width // (16 * LANES)
    return pl.pallas_call(
        end_state_kernel,
        out_shape=(
            pltpu.HBM((length, channels), BF16),
            pltpu.HBM((length, channels), BF16),
            pltpu.HBM(b.shape, BF16),
            pltpu.HBM((length, logits.shape[0]), F32),
            pltpu.HBM((blocks - 1, groups, STATE_WIDTH, width), F32),
            shape_of((pieces, 24, LANES), BF16),
        ),
        in_specs=[VMEM] * 9,
        out_specs=(VMEM,) * 6,
        scratch_shapes=[pltpu.VMEM((8 + length, LANES), F32)],
        compiler_params=limit(12),
        name="end_states",
    )(x, b, held(tail), xf, bf, logits, extra, bias, rate)


def chain_kernel(parts_ref, out_ref):
    peers = parts_ref.shape[0]

    def one(j, state):
        out_ref[j] = state.astype(BF16)
        logs = parts_ref[j, 16:24, :].astype(F32)
        factor = jnp.exp(logs[0:1] + logs[1:2] + logs[2:3])
        return state * factor + parts_ref[j, 0:16, :].astype(F32)

    lax.fori_loop(0, peers, one, jnp.zeros((16, LANES), F32), unroll=8)


def chain(parts):
    return pl.pallas_call(
        chain_kernel,
        out_shape=shape_of((parts.shape[0], 16, LANES), BF16),
        in_specs=[VMEM],
        out_specs=VMEM,
        compiler_params=limit(4),
        name="chain",
    )(held(parts))


def local_kernel(c_ref, tail_ref, cf_ref, bc_ref, xdt_ref, xc_ref, running_ref, direct_ref, cc_ref, y_ref, rows_ref):
    length, channels = xdt_ref.shape
    margin = cf_ref.shape[0] - 1
    groups = bc_ref.shape[1] // STATE_WIDTH
    width = channels // groups
    heads = width // HEAD_DIM
    offset = channels + groups * STATE_WIDTH
    for c in range(0, groups * STATE_WIDTH, LANES):
        cols = slice(c, c + LANES)
        fill_rows(rows_ref, tail_ref, c_ref, cols, offset, length)
        cc_ref[:, cols] = conv_cols(rows_ref, cf_ref[:, cols].astype(F32), length, margin).astype(BF16)
    t = lax.broadcasted_iota(jnp.int32, (BLOCK, BLOCK), 0)
    s = lax.broadcasted_iota(jnp.int32, (BLOCK, BLOCK), 1)
    causal = t >= s
    first_head = lax.broadcasted_iota(jnp.int32, (BLOCK, LANES), 1) < HEAD_DIM
    for i in range(length // BLOCK):
        rows = slice(i * BLOCK, (i + 1) * BLOCK)
        running = running_ref[rows, :]
        padded = jnp.concatenate([running, jnp.zeros((BLOCK, BLOCK - running.shape[1]), F32)], axis=1)
        across = padded.T
        for g in range(groups):
            wide = slice(g * STATE_WIDTH, (g + 1) * STATE_WIDTH)
            products = dot(cc_ref[rows, wide], bc_ref[rows, wide], ((1,), (1,)))
            products = jnp.where(causal, products, 0.0)
            for p in range(width // LANES):
                cols = slice(g * width + p * LANES, g * width + (p + 1) * LANES)
                pair = xdt_ref[rows, cols]
                total = direct_ref[:, cols] * xc_ref[rows, cols].astype(F32)
                for q in range(LANES // HEAD_DIM):
                    h = g * heads + p * (LANES // HEAD_DIM) + q
                    spread = running[:, h : h + 1] - across[h : h + 1, :]
                    weights = (products * jnp.exp(jnp.where(causal, spread, 0.0))).astype(BF16)
                    keep = first_head if q == 0 else ~first_head
                    total = total + dot(weights, jnp.where(keep, pair, jnp.zeros_like(pair)))
                y_ref[rows, cols] = total


def local_outputs(c, tail, cf, bc, xdt, xc, running, direct):
    length, channels = xdt.shape
    return pl.pallas_call(
        local_kernel,
        out_shape=(pltpu.HBM(c.shape, BF16), pltpu.HBM((length, channels), F32)),
        in_specs=[VMEM] * 8,
        out_specs=(VMEM, VMEM),
        scratch_shapes=[pltpu.VMEM((8 + length, LANES), F32)],
        compiler_params=limit(12),
        name="local_outputs",
    )(c, tail, cf, bc, xdt, xc, running, direct)


def project_kernel(y_ref, cc_ref, states_ref, incoming_ref, running_ref, gate_ref, scale_ref, w_hbm, out_ref, w_ref, rows_ref, sem):
    copy = pltpu.make_async_copy(w_hbm, w_ref, sem)
    copy.start()
    length, channels = y_ref.shape
    groups = cc_ref.shape[1] // STATE_WIDTH
    width = channels // groups
    heads = width // HEAD_DIM
    tiles = width // LANES
    for g in range(groups):
        here = slice(g * width, (g + 1) * width)
        wide = slice(g * STATE_WIDTH, (g + 1) * STATE_WIDTH)
        lines = []
        for n in range(STATE_WIDTH // 16):
            at = (g * (STATE_WIDTH // 16) + n) * tiles
            lines.append(jnp.concatenate([incoming_ref[at + p] for p in range(tiles)], axis=1))
        incoming = jnp.concatenate(lines, axis=0).astype(F32)
        started = jnp.zeros((1, running_ref.shape[1]), F32)
        for i in range(length // BLOCK):
            rows = slice(i * BLOCK, (i + 1) * BLOCK)
            running = running_ref[rows, :]
            if i == 0:
                state = incoming
            else:
                state = states_ref[i - 1, g] + incoming * spread_heads(jnp.exp(started), g, heads, width)
            started = started + running[BLOCK - 1 : BLOCK]
            read = dot(cc_ref[rows, wide], state.astype(BF16)) * spread_heads(jnp.exp(running), g, heads, width)
            gated = (y_ref[rows, here] + read) * silu(gate_ref[rows, here].astype(F32))
            power = jnp.mean(gated * gated, axis=1, keepdims=True)
            normed = gated * lax.rsqrt(power + EPS) * scale_ref[:, here].astype(F32)
            rows_ref[rows, here] = normed.astype(BF16)
    copy.wait()
    out_ref[...] = dot(rows_ref[...], w_ref[...]).astype(BF16)


def projected(y, cc, states, incoming, running, gate, scale, w):
    length, channels = y.shape
    return pl.pallas_call(
        project_kernel,
        out_shape=shape_of((length, w.shape[1]), BF16),
        in_specs=[VMEM] * 7 + [ANY],
        out_specs=VMEM,
        scratch_shapes=[
            pltpu.VMEM(w.shape, BF16),
            pltpu.VMEM((length, channels), BF16),
            pltpu.SemaphoreType.DMA,
        ],
        compiler_params=limit(20),
        name="projected",
    )(y, cc, states, held(incoming), running, gate, scale, *far_off(w))


def slots_kernel(capacity, routes_ref, slots_ref, count_ref):
    def clear(e, carry):
        count_ref[e] = 0
        return carry

    lax.fori_loop(0, count_ref.shape[0], clear, 0, unroll=8)

    def one(r, carry):
        for k in range(routes_ref.shape[0]):
            e = routes_ref[k, r]
            used = count_ref[e]
            count_ref[e] = used + 1
            slots_ref[k, r] = e * capacity + used
        return carry

    lax.fori_loop(0, routes_ref.shape[1], one, 0, unroll=4)


def slot_layout(routes, capacity, experts):
    return pl.pallas_call(
        lambda *refs: slots_kernel(capacity, *refs),
        out_shape=shape_of(routes.shape, jnp.int32),
        in_specs=[SMEM],
        out_specs=SMEM,
        scratch_shapes=[pltpu.SMEM((experts,), jnp.int32)],
        compiler_params=limit(1),
        name="slot_layout",
    )(routes)


def layer_norm(values, gain_row, bias_row):
    mean_value = jnp.mean(values, axis=-1, keepdims=True)
    centred = values - mean_value
    spread = jnp.mean(centred * centred, axis=-1, keepdims=True)
    return centred * lax.rsqrt(spread + EPS) * gain_row + bias_row


def middle_kernel(top_count, parts_ref, residual_ref, gain_ref, bias_ref, slots_ref, middle_ref, out_ref, blocks_ref):
    rows_here, width = residual_ref.shape
    chunks = width // LANES
    for r in range(0, rows_here, 16):
        rows = slice(r, r + 16)
        mixed = parts_ref[0, rows, :].astype(F32)
        for k in range(1, parts_ref.shape[0]):
            mixed = mixed + parts_ref[k, rows, :].astype(F32)
        values = layer_norm(ALPHA * residual_ref[rows, :].astype(F32) + mixed, gain_ref[...], bias_ref[...])
        for c in range(chunks):
            blocks_ref[pl.ds(r * chunks + c, 16, stride=chunks), :] = values[:, c * LANES : (c + 1) * LANES]

    def one(r, carry):
        at = pl.multiple_of(r * chunks, 16)
        block = blocks_ref[pl.ds(at, chunks), :].astype(BF16)
        middle_ref[r] = block
        for k in range(top_count):
            out_ref[slots_ref[k, r]] = block
        return carry

    lax.fori_loop(0, rows_here, one, 0, unroll=4)


def middle_rows(parts, residual, gain, bias, slots, top_count, slot_total):
    rows_here, width = residual.shape
    chunks = width // LANES
    return pl.pallas_call(
        lambda *refs: middle_kernel(top_count, *refs),
        out_shape=(
            shape_of((rows_here, chunks, LANES), BF16),
            shape_of((slot_total, chunks, LANES), BF16),
        ),
        in_specs=[VMEM] * 4 + [SMEM],
        out_specs=(VMEM, VMEM),
        scratch_shapes=[pltpu.VMEM((rows_here * chunks, LANES), F32)],
        compiler_params=limit(8),
        name="middle_rows",
    )(held(parts), residual, gain, bias, slots)


def expert_kernel(arrived_ref, *refs):
    pieces = refs[:-6]
    out_ref, blocks_ref, x_ref, hidden_ref, buffer_ref, sem = refs[-6:]
    slots, chunks, _ = arrived_ref.shape
    width = chunks * LANES
    quarters, _, units = buffer_ref.shape
    copies = []
    for n, source in enumerate(pieces):
        size = source.shape[0]
        own = n < 3
        quarter = 0 if own else 1 + (n - 3) // 2
        start = n * width if own else (n - 3) % 2 * size
        copies.append((quarter, pltpu.make_async_copy(source, buffer_ref.at[quarter, pl.ds(start, size)], sem.at[n])))
    for _, copy in copies:
        copy.start()
    for s in range(0, slots, 16):
        blocks_ref[s * chunks : (s + 16) * chunks, :] = arrived_ref[s : s + 16].reshape(16 * chunks, LANES).astype(F32)
    for c in range(chunks):
        x_ref[:, c * LANES : (c + 1) * LANES] = blocks_ref[pl.ds(c, slots, stride=chunks), :].astype(BF16)
    for q in range(quarters):
        for quarter, copy in copies:
            if quarter == q:
                copy.wait()
        gate = dot(x_ref[...], buffer_ref[q, :width, :])
        up = dot(x_ref[...], buffer_ref[q, width : 2 * width, :])
        hidden_ref[:, q * units : (q + 1) * units] = (silu(gate) * up).astype(BF16)
    step = 512
    for n in range(0, width, step):
        total = None
        for q in range(quarters):
            down = buffer_ref[q, 2 * width + n : 2 * width + n + step, :]
            part = dot(hidden_ref[:, q * units : (q + 1) * units], down, ((1,), (1,)))
            total = part if total is None else total + part
        for c in range(step // LANES):
            blocks_ref[pl.ds(n // LANES + c, slots, stride=chunks), :] = total[:, c * LANES : (c + 1) * LANES]
    for s in range(0, slots, 16):
        out_ref[s : s + 16] = blocks_ref[s * chunks : (s + 16) * chunks, :].astype(BF16).reshape(16, chunks, LANES)


def expert_answers(arrived, own, packs):
    slots, chunks, _ = arrived.shape
    width = chunks * LANES
    units = own[0].shape[1]
    pieces = [*own, *packs]
    return pl.pallas_call(
        expert_kernel,
        out_shape=shape_of(arrived.shape, BF16),
        in_specs=[VMEM] + [ANY] * len(pieces),
        out_specs=VMEM,
        scratch_shapes=[
            pltpu.VMEM((slots * chunks, LANES), F32),
            pltpu.VMEM((slots, width), BF16),
            pltpu.VMEM((slots, 4 * units), BF16),
            pltpu.VMEM((4, 3 * width, units), BF16),
            pltpu.SemaphoreType.DMA((len(pieces),)),
        ],
        compiler_params=limit(36),
        name="expert_answers",
    )(held(arrived), *far_off(*pieces))


def pack_kernel(gate_ref, up_ref, down_ref, first_ref, second_ref, stage_ref, into, out):
    width = gate_ref.shape[0]
    half = width // 2
    sources = (
        gate_ref.at[pl.ds(0, half)],
        gate_ref.at[pl.ds(half, half)],
        up_ref.at[pl.ds(0, half)],
        up_ref.at[pl.ds(half, half)],
        down_ref.at[pl.ds(0, half)],
        down_ref.at[pl.ds(half, half)],
    )
    loads = [pltpu.make_async_copy(source, stage_ref.at[n], into.at[n]) for n, source in enumerate(sources)]
    stores = []
    for n in range(len(sources)):
        target = first_ref if n < 3 else second_ref
        stores.append(pltpu.make_async_copy(stage_ref.at[n], target.at[pl.ds(n % 3 * half, half)], out.at[n]))
    for load in loads:
        load.start()
    for load, store in zip(loads, stores):
        load.wait()
        store.start()
    for store in stores:
        store.wait()


def packed(gate, up, down):
    width, units = gate.shape
    both = pltpu.HBM((width * 3 // 2, units), BF16)
    return pl.pallas_call(
        pack_kernel,
        out_shape=(both, both),
        in_specs=[ANY] * 3,
        out_specs=(ANY, ANY),
        scratch_shapes=[
            pltpu.VMEM((6, width // 2, units), BF16),
            pltpu.SemaphoreType.DMA((6,)),
            pltpu.SemaphoreType.DMA((6,)),
        ],
        compiler_params=limit(8),
        name="packed",
    )(*far_off(gate, up, down))


def tail_kernel(x_ref, b_ref, c_ref, out_ref, sem):
    rows = out_ref.shape[0]
    copies = []
    start = 0
    for n, ref in enumerate((x_ref, b_ref, c_ref)):
        length, width = ref.shape
        source = ref.at[pl.ds(length - rows, rows)]
        copies.append(pltpu.make_async_copy(source, out_ref.at[:, pl.ds(start, width)], sem.at[n]))
        start += width
    for copy in copies:
        copy.start()
    for copy in copies:
        copy.wait()


def last_rows(x, b, c, rows):
    return pl.pallas_call(
        tail_kernel,
        out_shape=near((rows, x.shape[1] + b.shape[1] + c.shape[1]), BF16),
        in_specs=[ANY] * 3,
        out_specs=VMEM,
        scratch_shapes=[pltpu.SemaphoreType.DMA((3,))],
        compiler_params=limit(1),
        name="last_rows",
    )(*far_off(x, b, c))


def final_kernel(top_count, returned_ref, middle_ref, slots_ref, weights_ref, gain_ref, bias_ref, out_ref, blocks_ref):
    rows_here, chunks, _ = middle_ref.shape

    def one(r, carry):
        total = returned_ref[slots_ref[0, r]].astype(F32) * weights_ref[0, r]
        for k in range(1, top_count):
            total = total + returned_ref[slots_ref[k, r]].astype(F32) * weights_ref[k, r]
        start = pl.multiple_of(r * chunks, 16)
        blocks_ref[pl.ds(start, chunks), :] = ALPHA * middle_ref[r].astype(F32) + total
        return carry

    lax.fori_loop(0, rows_here, one, 0, unroll=4)
    for r in range(0, rows_here, 16):
        values = jnp.concatenate(
            [blocks_ref[pl.ds(r * chunks + c, 16, stride=chunks), :] for c in range(chunks)], axis=1
        )
        out_ref[r : r + 16, :] = layer_norm(values, gain_ref[...], bias_ref[...]).astype(BF16)


def final_rows(returned, middle, slots, weights, gain, bias, top_count):
    rows_here, chunks, _ = middle.shape
    return pl.pallas_call(
        lambda *refs: final_kernel(top_count, *refs),
        out_shape=shape_of((rows_here, chunks * LANES), BF16),
        in_specs=[VMEM, VMEM, SMEM, SMEM, VMEM, VMEM],
        out_specs=VMEM,
        scratch_shapes=[pltpu.VMEM((rows_here * chunks, LANES), F32)],
        compiler_params=limit(8),
        name="final_rows",
    )(held(returned), middle, slots, weights, gain, bias)


def turned_by(value, distance):
    peers = lax.axis_size("tp")
    return lax.ppermute(value, "tp", [(i, (i + distance) % peers) for i in range(peers)])


def exchanged(value, axis):
    return lax.all_to_all(value, axis, split_axis=0, concat_axis=0, tiled=True)


def shards(
    head_input_values,
    group_input_vectors,
    group_readout_vectors,
    output_gate_values,
    step_size_logits,
    extra_log_decay,
    head_input_filter,
    input_vector_filter,
    readout_vector_filter,
    step_size_bias,
    head_rate_logarithm,
    direct_path_weight,
    group_norm_scale,
    mixer_output_weight,
    residual,
    first_norm_scale,
    first_norm_bias,
    routes,
    routing_weight,
    expert_gate_weight,
    expert_up_weight,
    expert_down_weight,
    final_norm_scale,
    final_norm_bias,
):
    devices = lax.axis_size(SP)
    experts = expert_gate_weight.shape[0] * devices
    rows_here, top_count = routes.shape
    width = residual.shape[1]
    capacity = 5

    own = (expert_gate_weight[0], expert_up_weight[0], expert_down_weight[0])
    ending = last_rows(head_input_values, group_input_vectors, group_readout_vectors, 8)
    tail = lax.ppermute(ending, SP, [(i, i + 1) for i in range(devices - 1)])
    first, second = packed(*own)
    first_behind = turned_by(first, 1)
    first_ahead = turned_by(first, -1)
    second_behind = turned_by(second, 1)
    second_ahead = turned_by(second, -1)
    xc, xdt, bc, running, states, message = end_states(
        head_input_values,
        group_input_vectors,
        tail,
        head_input_filter,
        input_vector_filter,
        step_size_logits.T,
        extra_log_decay.T,
        step_size_bias[None],
        head_rate_logarithm[None],
    )
    met = exchanged(message, SP)
    slots = slot_layout(routes.T, capacity, experts)
    direct = jnp.repeat(direct_path_weight, HEAD_DIM)[None]
    cc, y = local_outputs(group_readout_vectors, tail, readout_vector_filter, bc, xdt, xc, running, direct)
    incoming = exchanged(chain(met), SP)
    sums = projected(
        y, cc, states, incoming, running, output_gate_values, group_norm_scale[None], mixer_output_weight
    )
    peers = lax.axis_size("tp")
    parts = exchanged(sums.reshape(peers, rows_here, width), "tp")
    first_behind, second_ahead, parts = lax.optimization_barrier((first_behind, second_ahead, parts))
    first_far = turned_by(first_behind, 1)
    second_far = turned_by(second_ahead, -1)
    middle, outgoing = middle_rows(
        parts, residual, first_norm_scale[None], first_norm_bias[None], slots, top_count, experts * capacity
    )
    chunks = width // LANES
    arrived = exchanged(outgoing.reshape(experts, capacity * chunks, LANES), SP)
    answers = expert_answers(
        arrived.reshape(experts * capacity, chunks, LANES),
        own,
        (first_behind, second_behind, first_ahead, second_ahead, first_far, second_far),
    )
    returned = exchanged(answers.reshape(experts, capacity * chunks, LANES), SP)
    return final_rows(
        returned.reshape(experts * capacity, chunks, LANES),
        middle,
        slots,
        routing_weight.T,
        final_norm_scale[None],
        final_norm_bias[None],
        top_count,
    )


def solution(mesh):
    placed = (
        P(SP, "tp"),
        P(SP, "tp"),
        P(SP, "tp"),
        P(SP, "tp"),
        P(SP, "tp"),
        P(SP, "tp"),
        P(None, "tp"),
        P(None, "tp"),
        P(None, "tp"),
        P("tp"),
        P("tp"),
        P("tp"),
        P("tp"),
        P("tp", None),
        P(SP_TP, None),
        P(),
        P(),
        P(SP_TP, None),
        P(SP_TP, None),
        P(SP, None, "tp"),
        P(SP, None, "tp"),
        P(SP, None, "tp"),
        P(),
        P(),
    )
    return jax.shard_map(shards, mesh=mesh, in_specs=placed, out_specs=P(SP_TP, None), check_vma=False)
```

time: 399 us -> 252 us (0.63)
  local copies, waits for them, and re-layouts: 87.6 us -> 10 us
  waiting for transfers between devices: 139 us -> 103 us
  Pallas kernels: 0 us -> 33.6 us
  matrix products: 25.7 us -> 0 us
  other arithmetic: 22.4 us -> 0 us
  blocking collectives: 88.5 us -> 71.9 us
  between operations: 13.6 us -> 0.26 us
  starting transfers between devices: 20.3 us -> 31.3 us
    ppermute x3 -> x7, waiting for transfers between devices: 0.01 us -> 85.1 us  [the longest x6 81.9 us: turned_by(): lax.ppermute(value, 'tp', [(i, (i + distance) % peers) for i in range(pee...]
    all_to_all x2 -> x3, waiting for transfers between devices: 86 us -> 18.2 us  [exchanged(): return lax.all_to_all(value, axis, split_axis=0, concat_axis=0, tiled=True)]
    all_gather x3 -> x0, waiting for transfers between devices: 52.7 us -> none  [the longest x2 34.8 us: prefix_by_axis(): lax.all_gather(part.astype(kind), axis)]
    dynamic_update_slice x3 -> x0, local copies, waits for them, and re-layouts: 41.5 us -> none  [shards(): lax.scan(block_pass, start_state, (step_scaled_inputs.reshape(block_list,...]
    pallas_call x0 -> x10, Pallas kernels: none -> 33.6 us  [the longest x1 7.52 us: expert_answers(): pl.pallas_call(expert_kernel, out_shape=shape_of(arrived.shape, BF16), in...]
    all_gather x4 -> x0, blocking collectives: 29.9 us -> none  [prefix_by_axis(): lax.all_gather(part.astype(kind), axis)]
    dot_general x16 -> x0, matrix products: 25.7 us -> none  [the longest x1 8.13 us: expert_output(): jnp.einsum('senf,edf->send', hidden, weight_down, preferred_element_type=...]
    reshape x8 -> x0, local copies, waits for them, and re-layouts: 13.5 us -> none  [the longest x1 3.92 us: shards(): within_block_output.reshape(length, groups_here, repeat_count, HEAD_DIM)]
  transfers between devices with their start and end apart: 8 -> 10, of which waited for: 5 -> 8; matrix products, arithmetic and copies ran while one was open for 11% -> 0% of each run, Pallas kernels for 0% -> 6%
where the time goes in v1:
time: 252 us; the launch traced here: 250 us
  waiting for transfers between devices  103 us (41%)
  blocking collectives  71.9 us (29%)
  Pallas kernels  33.6 us (13%)
  starting transfers between devices  31.3 us (12%)
  local copies, waits for them, and re-layouts  10 us (4%)
    ppermute x6, waiting for transfers between devices, turned_by(): lax.ppermute(value, 'tp', [(i, (i + distance) % peers) for i in range(pee...  81.9 us
    all_to_all x2, blocking collectives, exchanged(): return lax.all_to_all(value, axis, split_axis=0, concat_axis=0, tiled=True)  71.9 us
    all_to_all x3, starting transfers between devices, exchanged(): return lax.all_to_all(value, axis, split_axis=0, concat_axis=0, tiled=True)  20.8 us
    all_to_all x3, waiting for transfers between devices, exchanged(): return lax.all_to_all(value, axis, split_axis=0, concat_axis=0, tiled=True)  18.2 us
    unnamed x62, local copies, waits for them, and re-layouts  9.86 us
    ppermute x6, starting transfers between devices, turned_by(): lax.ppermute(value, 'tp', [(i, (i + distance) % peers) for i in range(pee...  8.65 us
    pallas_call x1, Pallas kernels, expert_answers(): pl.pallas_call(expert_kernel, out_shape=shape_of(arrived.shape, BF16), in...  7.52 us
    pallas_call x1, Pallas kernels, projected(): pl.pallas_call(project_kernel, out_shape=shape_of((length, w.shape[1]), B...  6.77 us
  transfers between devices with their start and end apart: 10, of which 8 were waited for; matrix products, arithmetic and copies ran while one was open for 0% of the time, Pallas kernels for 6%

profile of v1, /device:TPU:8, one launch (start us, length us, event | category | flops | bytes accessed | tf_op | source)
XLA Modules:
  0.0 250.4 jit_solution(7151427138565968888)
XLA Ops:
  0.8 1.9 collective-permute-start.2
  2.8 3.2 %collective-permute-done.2.tail_ref = bf16[8,1536]{1,0:T(8,128)(2,1)S(1)} collective-permute-done((bf16[8,1536]{1,0:T(8,128)(2,1)S(1)}, bf16[8,1536]{1,0:T(8,128)(2,1)S(1)}, u32[]{:S(2)}, u32[]{:S(2)}) %collective-permute-start.2) | collective-permute-done | bytes 24608 | tf_op jit(solution)/shard_map/ppermute | solution.py:602
  11.1 4.4 %end_states.1 = (bf16[384,1024]{1,0:T(8,128)(2,1)}, bf16[384,1024]{1,0:T(8,128)(2,1)}, bf16[384,256]{1,0:T(8,128)(2,1)}, f32[384,16]{1,0:T(8,128)}, f32[2,2,128,...) custom-call(bf16[384,1024]{1,0:T(8,128)(2,1)S(1)} %copy-done, bf16[384,256]{1,0:T(8,128)(2,1)S(1)} %copy-done.6, ...), custom_call_target="tpu_custom_call" | custom-call | tf_op jit(solution)/shard_map/end_states/pallas_call | solution.py:177
  15.5 27.3 %all_to_all.25.parts_ref = bf16[64,24,128]{2,1,0:T(8,128)(2,1)S(1)} all-to-all(bf16[64,24,128]{2,1,0:T(8,128)(2,1)S(1)} %get-tuple-element.29), channel_id=1, replica_groups=mesh['sp'=64,'tp'=4] {'sp'}, dimensions={0} | all-to-all | bytes 786432 | tf_op jit(solution)/shard_map/all_to_all | solution.py:565
  43.7 5.9 %all-to-all-start.1 = ((bf16[64,16,128]{2,1,0:T(8,128)(2,1)}), bf16[64,16,128]{2,1,0:T(8,128)(2,1)S(1)}, u32[]{:S(2)}, u32[]{:S(2)}) async-start(bf16[64,16,128]{2,1,0:T(8,128)(2,1)} %chain.1), calls=%async_computation.1 | async-start | bytes 524288 | tf_op jit(solution)/shard_map/all_to_all | solution.py:565
  49.7 2.9 %packed.1 = (bf16[3072,256]{1,0:T(8,128)(2,1)}, bf16[3072,256]{1,0:T(8,128)(2,1)}) custom-call(bf16[2048,256]{1,0:T(8,128)(2,1)} %bitcast.31, bf16[2048,256]{1,0:T(8,128)(2,1)} %bitcast.33, bf16[2048,256]{1,0:T(8,128)(2,1)} %bitcast.35), custom_call_target="tpu_custom_call" | custom-call | tf_op jit(solution)/shard_map/packed/pallas_call | solution.py:485
  52.7 1.6 collective-permute-start
  54.2 1.7 collective-permute-start.1
  57.3 2.9 %local_outputs.1 = (bf16[384,256]{1,0:T(8,128)(2,1)}, f32[384,1024]{1,0:T(8,128)}) custom-call(bf16[384,256]{1,0:T(8,128)(2,1)S(1)} %copy-done.7, bf16[8,1536]{1,0:T(8,128)(2,1)S(1)} %collective-permute-done.2.tail_ref, bf16[4,256]{1,0:T(4,128)(2,1)S(1)} %copy-done.20, bf16[384,256]{1,0:T(8,128)(2,1)S(1)} %copy-done.10, bf16[384,1024]{1,0:T(8,128)(2,1)S(1)} %copy-done.5, ...), custom_call_target="tpu_custom_call" | custom-call | tf_op jit(solution)/shard_map/local_outputs/pallas_call | solution.py:257
  64.2 6.8 %projected.1 = bf16[384,2048]{1,0:T(8,128)(2,1)} custom-call(f32[384,1024]{1,0:T(8,128)S(1)} %copy-done.1, bf16[384,256]{1,0:T(8,128)(2,1)S(1)} %copy-done.11, f32[2,2,128,512]{3,2,1,0:T(8,128)S(1)} %copy-done.2, bf16[64,16,128]{2,1,0:T(8,128)(2,1)S(1)} %all-to-all-done.1.incoming_ref, f32[384,16]{1,0:T(8,128)S(1)} %copy-done.8, ...), custom_call_target="tpu_custom_call" | custom-call | tf_op jit(solution)/shard_map/projected/pallas_call | solution.py:304
  71.0 4.4 %all-to-all-start.2 = ((bf16[4,96,2048]{2,1,0:T(8,128)(2,1)}), bf16[4,96,2048]{2,1,0:T(8,128)(2,1)S(1)}, u32[]{:S(2)}, u32[]{:S(2)}) async-start(bf16[4,96,2048]{2,1,0:T(8,128)(2,1)} %bitcast.7), calls=%async_computation.2 | async-start | bytes 3145728 | tf_op jit(solution)/shard_map/all_to_all | solution.py:565
  75.4 2.2 slot_layout.1.refs_4_.refs_2_
  77.7 13.9 %collective-permute-done.refs_3_ = bf16[3072,256]{1,0:T(8,128)(2,1)} collective-permute-done((bf16[3072,256]{1,0:T(8,128)(2,1)}, bf16[3072,256]{1,0:T(8,128)(2,1)}, u32[]{:S(2)}, u32[]{:S(2)}) %collective-permute-start) | collective-permute-done | bytes 1572896 | tf_op jit(solution)/shard_map/ppermute | solution.py:561
  91.8 16.6 %all-to-all-done.2.refs_0_ = bf16[4,96,2048]{2,1,0:T(8,128)(2,1)S(1)} async-done(((bf16[4,96,2048]{2,1,0:T(8,128)(2,1)}), bf16[4,96,2048]{2,1,0:T(8,128)(2,1)S(1)}, u32[]{:S(2)}, u32[]{:S(2)}) %all-to-all-start.2) | async-done | bytes 1572896 | tf_op jit(solution)/shard_map/all_to_all | solution.py:565
  108.4 2.7 %middle_rows.1 = (bf16[96,16,128]{2,1,0:T(8,128)(2,1)S(1)}, bf16[320,16,128]{2,1,0:T(8,128)(2,1)}) custom-call(bf16[4,96,2048]{2,1,0:T(8,128)(2,1)S(1)} %all-to-all-done.2.refs_0_, bf16[96,2048]{1,0:T(8,128)(2,1)S(1)} %copy-done.9, f32[1,2048]{1,0:T(1,128)S(1)} %bitcast.23, f32[1,2048]{1,0:T(1,128)S(1)} %bitcast.24, s32[2,96]{1,0:T(2,128)S(1)} %slot_layout.1.refs_4_.refs_2_), custom_call_target="tpu_custom_call" | custom-call | tf_op jit(solution)/shard_map/middle_rows/pallas_call | solution.py:382
  111.1 10.4 %all-to-all-start.3 = ((bf16[64,80,128]{2,1,0:T(8,128)(2,1)}), bf16[64,80,128]{2,1,0:T(8,128)(2,1)S(1)}, u32[]{:S(2)}, u32[]{:S(2)}) async-start(bf16[64,80,128]{2,1,0:T(8,128)(2,1)} %bitcast.11), calls=%async_computation.3 | async-start | bytes 2621440 | tf_op jit(solution)/shard_map/all_to_all | solution.py:565
  121.6 2.0 collective-permute-start.4
  124.8 2.1 collective-permute-start.6
  126.9 32.2 %collective-permute-done.4.refs_5_ = bf16[3072,256]{1,0:T(8,128)(2,1)S(1)} collective-permute-done((bf16[3072,256]{1,0:T(8,128)(2,1)}, bf16[3072,256]{1,0:T(8,128)(2,1)S(1)}, u32[]{:S(2)}, u32[]{:S(2)}) %collective-permute-start.4) | collective-permute-done | bytes 1572896 | tf_op jit(solution)/shard_map/ppermute | solution.py:561
  159.1 3.0 %collective-permute-done.3.refs_4_ = bf16[3072,256]{1,0:T(8,128)(2,1)S(1)} collective-permute-done((bf16[3072,256]{1,0:T(8,128)(2,1)S(1)}, bf16[3072,256]{1,0:T(8,128)(2,1)S(1)}, u32[]{:S(2)}, u32[]{:S(2)}) %collective-permute-start.3) | collective-permute-done | bytes 1572896 | tf_op jit(solution)/shard_map/ppermute | solution.py:561
  162.1 32.6 %collective-permute-done.5.refs_7_ = bf16[3072,256]{1,0:T(8,128)(2,1)S(1)} collective-permute-done((bf16[3072,256]{1,0:T(8,128)(2,1)}, bf16[3072,256]{1,0:T(8,128)(2,1)S(1)}, u32[]{:S(2)}, u32[]{:S(2)}) %collective-permute-start.5) | collective-permute-done | bytes 1572896 | tf_op jit(solution)/shard_map/ppermute | solution.py:561
  195.9 7.5 %expert_answers.1 = bf16[320,16,128]{2,1,0:T(8,128)(2,1)S(1)} custom-call(bf16[320,16,128]{2,1,0:T(8,128)(2,1)S(1)} %bitcast.19, bf16[2048,256]{1,0:T(8,128)(2,1)} %bitcast.32, bf16[2048,256]{1,0:T(8,128)(2,1)} %bitcast.34, bf16[2048,256]{1,0:T(8,128)(2,1)} %bitcast.36, bf16[3072,256]{1,0:T(8,128)(2,1)} %collective-permute-done.refs_3_, ...), custom_call_target="tpu_custom_call" | custom-call | tf_op jit(solution)/shard_map/expert_answers/pallas_call | solution.py:440
  203.5 44.6 %all_to_all.26 = bf16[64,80,128]{2,1,0:T(8,128)(2,1)S(1)} all-to-all(bf16[64,80,128]{2,1,0:T(8,128)(2,1)S(1)} %bitcast.20), channel_id=1, replica_groups=mesh['sp'=64,'tp'=4] {'sp'}, dimensions={0} | all-to-all | bytes 2621440 | tf_op jit(solution)/shard_map/all_to_all | solution.py:565
  248.1 2.3 final_rows.1
  (73 shorter events, 14.8 us)
Async XLA Ops:
  0.8 5.1 %collective-permute-start.2 = (bf16[8,1536]{1,0:T(8,128)(2,1)S(1)}, bf16[8,1536]{1,0:T(8,128)(2,1)S(1)}, u32[]{:S(2)}, u32[]{:S(2)}) collective-permute-start(bf16[8,1536]{1,0:T(8,128)(2,1)S(1)} %last_rows.1), channel_id=1, source_target_pairs={{0,4},{4,8},{8,12},{12,16},{16,20},{20,24},{24,28},{28,32},{32,36}... | collective-permute-start | bytes 73736 | tf_op jit(solution)/shard_map/ppermute | solution.py:602
  43.7 18.1 %all-to-all-start.1 = ((bf16[64,16,128]{2,1,0:T(8,128)(2,1)}), bf16[64,16,128]{2,1,0:T(8,128)(2,1)S(1)}, u32[]{:S(2)}, u32[]{:S(2)}) async-start(bf16[64,16,128]{2,1,0:T(8,128)(2,1)} %chain.1), calls=%async_computation.1 | async-start | bytes 524288 | tf_op jit(solution)/shard_map/all_to_all | solution.py:565
  49.7 6.5 %copy-start.4 = (bf16[384,1024]{1,0:T(8,128)(2,1)S(1)}, bf16[384,1024]{1,0:T(8,128)(2,1)}, u32[]{:S(2)}) copy-start(bf16[384,1024]{1,0:T(8,128)(2,1)} %get-tuple-element.24.xc_ref) | copy-start | bytes 2359300
  49.7 6.5 %copy-start.7 = (bf16[384,256]{1,0:T(8,128)(2,1)S(1)}, bf16[384,256]{1,0:T(8,128)(2,1)}, u32[]{:S(2)}) copy-start(bf16[384,256]{1,0:T(8,128)(2,1)} %c_ref.3) | copy-start | bytes 589828
  49.7 6.5 %copy-start.8 = (f32[384,16]{1,0:T(8,128)S(1)}, f32[384,16]{1,0:T(8,128)}, u32[]{:S(2)}) copy-start(f32[384,16]{1,0:T(8,128)} %get-tuple-element.25.running_ref) | copy-start | bytes 73732
  52.6 9.2 %copy-start.2 = (f32[2,2,128,512]{3,2,1,0:T(8,128)S(1)}, f32[2,2,128,512]{3,2,1,0:T(8,128)}, u32[]{:S(2)}) copy-start(f32[2,2,128,512]{3,2,1,0:T(8,128)} %get-tuple-element.28.states_ref) | copy-start | bytes 3145732
  52.7 9.2 %copy-start.3 = (bf16[384,1024]{1,0:T(8,128)(2,1)S(1)}, bf16[384,1024]{1,0:T(8,128)(2,1)}, u32[]{:S(2)}) copy-start(bf16[384,1024]{1,0:T(8,128)(2,1)} %gate_ref.1) | copy-start | bytes 2359300
  52.7 38.9 %collective-permute-start = (bf16[3072,256]{1,0:T(8,128)(2,1)}, bf16[3072,256]{1,0:T(8,128)(2,1)}, u32[]{:S(2)}, u32[]{:S(2)}) collective-permute-start(bf16[3072,256]{1,0:T(8,128)(2,1)} %get-tuple-element.20), channel_id=1, source_target_pairs={{0,1},{1,2},{2,3},{3,0},{4,5},{5,6},{6,7},{7,4},{8,9},{9,10},{10,1... | collective-permute-start | bytes 4718600 | tf_op jit(solution)/shard_map/ppermute | solution.py:561
  54.2 37.6 %collective-permute-start.1 = (bf16[3072,256]{1,0:T(8,128)(2,1)}, bf16[3072,256]{1,0:T(8,128)(2,1)}, u32[]{:S(2)}, u32[]{:S(2)}) collective-permute-start(bf16[3072,256]{1,0:T(8,128)(2,1)} %get-tuple-element.21), channel_id=1, source_target_pairs={{0,3},{1,0},{2,1},{3,2},{4,7},{5,4},{6,5},{7,6},{8,11},{9,8},{10,9... | collective-permute-start | bytes 4718600 | tf_op jit(solution)/shard_map/ppermute | solution.py:561
  71.0 37.5 %copy-start.9 = (bf16[96,2048]{1,0:T(8,128)(2,1)S(1)}, bf16[96,2048]{1,0:T(8,128)(2,1)}, u32[]{:S(2)}) copy-start(bf16[96,2048]{1,0:T(8,128)(2,1)} %refs_1_.1) | copy-start | bytes 1179652
  71.0 37.5 %copy-start.15 = (f32[2048]{0:T(1024)S(1)}, f32[2048]{0:T(1024)}, u32[]{:S(2)}) copy-start(f32[2048]{0:T(1024)} %param.39) | copy-start | bytes 24580
  71.0 37.4 %copy-start.16 = (f32[2048]{0:T(1024)S(1)}, f32[2048]{0:T(1024)}, u32[]{:S(2)}) copy-start(f32[2048]{0:T(1024)} %param.40) | copy-start | bytes 24580
  71.0 37.4 %all-to-all-start.2 = ((bf16[4,96,2048]{2,1,0:T(8,128)(2,1)}), bf16[4,96,2048]{2,1,0:T(8,128)(2,1)S(1)}, u32[]{:S(2)}, u32[]{:S(2)}) async-start(bf16[4,96,2048]{2,1,0:T(8,128)(2,1)} %bitcast.7), calls=%async_computation.2 | async-start | bytes 3145728 | tf_op jit(solution)/shard_map/all_to_all | solution.py:565
  111.1 12.5 %copy-start.30 = (bf16[3072,256]{1,0:T(8,128)(2,1)S(1)}, bf16[3072,256]{1,0:T(8,128)(2,1)}, u32[]{:S(2)}) copy-start(bf16[3072,256]{1,0:T(8,128)(2,1)} %get-tuple-element.21) | copy-start | bytes 4718596
  111.1 84.8 %all-to-all-start.3 = ((bf16[64,80,128]{2,1,0:T(8,128)(2,1)}), bf16[64,80,128]{2,1,0:T(8,128)(2,1)S(1)}, u32[]{:S(2)}, u32[]{:S(2)}) async-start(bf16[64,80,128]{2,1,0:T(8,128)(2,1)} %bitcast.11), calls=%async_computation.3 | async-start | bytes 2621440 | tf_op jit(solution)/shard_map/all_to_all | solution.py:565
  121.6 37.6 %collective-permute-start.4 = (bf16[3072,256]{1,0:T(8,128)(2,1)}, bf16[3072,256]{1,0:T(8,128)(2,1)S(1)}, u32[]{:S(2)}, u32[]{:S(2)}) collective-permute-start(bf16[3072,256]{1,0:T(8,128)(2,1)} %get-tuple-element.20), channel_id=1, source_target_pairs={{0,3},{1,0},{2,1},{3,2},{4,7},{5,4},{6,5},{7,6},{8,11},{9,8},{10,9... | collective-permute-start | bytes 4718600 | tf_op jit(solution)/shard_map/ppermute | solution.py:561
  123.6 38.5 %collective-permute-start.3 = (bf16[3072,256]{1,0:T(8,128)(2,1)S(1)}, bf16[3072,256]{1,0:T(8,128)(2,1)S(1)}, u32[]{:S(2)}, u32[]{:S(2)}) collective-permute-start(bf16[3072,256]{1,0:T(8,128)(2,1)S(1)} %copy-done.30), channel_id=1, source_target_pairs={{0,1},{1,2},{2,3},{3,0},{4,5},{5,6},{6,7},{7,4},{8,9},{9,10},{10,1... | collective-permute-start | bytes 4718600 | tf_op jit(solution)/shard_map/ppermute | solution.py:561
  123.7 71.0 %collective-permute-start.5 = (bf16[3072,256]{1,0:T(8,128)(2,1)}, bf16[3072,256]{1,0:T(8,128)(2,1)S(1)}, u32[]{:S(2)}, u32[]{:S(2)}) collective-permute-start(bf16[3072,256]{1,0:T(8,128)(2,1)} %collective-permute-done.refs_3_), channel_id=1, source_target_pairs={{0,1},{1,2},{2,3},{3,0},{4,5},{5,6},{6,7},{7,4},{8,9},{9,10},{10,1... | collective-permute-start | bytes 4718600 | tf_op jit(solution)/shard_map/ppermute | solution.py:561
  124.8 71.1 %collective-permute-start.6 = (bf16[3072,256]{1,0:T(8,128)(2,1)}, bf16[3072,256]{1,0:T(8,128)(2,1)}, u32[]{:S(2)}, u32[]{:S(2)}) collective-permute-start(bf16[3072,256]{1,0:T(8,128)(2,1)} %collective-permute-done.1.refs_6_), channel_id=1, source_target_pairs={{0,3},{1,0},{2,1},{3,2},{4,7},{5,4},{6,5},{7,6},{8,11},{9,8},{10,9... | collective-permute-start | bytes 4718600 | tf_op jit(solution)/shard_map/ppermute | solution.py:561
  159.1 35.6 %copy-start.25 = (bf16[3072,256]{1,0:T(8,128)(2,1)}, bf16[3072,256]{1,0:T(8,128)(2,1)S(1)}, u32[]{:S(2)}) copy-start(bf16[3072,256]{1,0:T(8,128)(2,1)S(1)} %collective-permute-done.4.refs_5_) | copy-start | bytes 4718596
  162.1 32.6 %copy-start.26 = (bf16[3072,256]{1,0:T(8,128)(2,1)}, bf16[3072,256]{1,0:T(8,128)(2,1)S(1)}, u32[]{:S(2)}) copy-start(bf16[3072,256]{1,0:T(8,128)(2,1)S(1)} %collective-permute-done.3.refs_4_) | copy-start | bytes 4718596
  203.4 44.7 %copy-start.17 = (f32[2048]{0:T(1024)S(1)}, f32[2048]{0:T(1024)}, u32[]{:S(2)}) copy-start(f32[2048]{0:T(1024)} %param.46) | copy-start | bytes 24580
  203.4 44.7 %copy-start.18 = (f32[2048]{0:T(1024)S(1)}, f32[2048]{0:T(1024)}, u32[]{:S(2)}) copy-start(f32[2048]{0:T(1024)} %param.47) | copy-start | bytes 24580
  203.5 44.6 %copy-start.21 = (f32[96,2]{0,1:T(2,128)S(1)}, f32[96,2]{0,1:T(2,128)}, u32[]{:S(2)}) copy-start(f32[96,2]{0,1:T(2,128)} %param.42) | copy-start | bytes 2308
  (17 other events, 45.9 us)

commit v2 on v1

--- a/solution.py
+++ b/solution.py
@@ -10,6 +10,7 @@
 STATE_WIDTH = 128
 BLOCK = 128
 LANES = 128
+PITCH = 20
 SP = "sp"
 SP_TP = ("sp", "tp")
 EPS = 1e-05
@@ -47,7 +48,7 @@
 
 
 def silu(v):
-    return v * (1.0 / (1.0 + jnp.exp(-v)))
+    return 0.5 * v * (1.0 + jnp.tanh(0.5 * v))
 
 
 def spread_heads(values, group, heads, width):
@@ -168,7 +169,7 @@
                 message_ref[at, 16:24, :] = logs[:, p * LANES : (p + 1) * LANES]
 
 
-def end_states(x, b, tail, xf, bf, logits, extra, bias, rate):
+def end_states(tail, x, b, xf, bf, logits, extra, bias, rate):
     length, channels = x.shape
     groups = b.shape[1] // STATE_WIDTH
     blocks = length // BLOCK
@@ -189,7 +190,7 @@
         scratch_shapes=[pltpu.VMEM((8 + length, LANES), F32)],
         compiler_params=limit(12),
         name="end_states",
-    )(x, b, held(tail), xf, bf, logits, extra, bias, rate)
+    )(*map(held, (x, b, tail, xf, bf, logits, extra, bias, rate)))
 
 
 def chain_kernel(parts_ref, out_ref):
@@ -215,7 +216,22 @@
     )(held(parts))
 
 
-def local_kernel(c_ref, tail_ref, cf_ref, bc_ref, xdt_ref, xc_ref, running_ref, direct_ref, cc_ref, y_ref, rows_ref):
+def local_kernel(
+    c_ref,
+    tail_ref,
+    cf_ref,
+    bc_ref,
+    xdt_ref,
+    xc_ref,
+    running_ref,
+    states_ref,
+    direct_ref,
+    gate_ref,
+    cc_ref,
+    fixed_ref,
+    factor_ref,
+    rows_ref,
+):
     length, channels = xdt_ref.shape
     margin = cf_ref.shape[0] - 1
     groups = bc_ref.shape[1] // STATE_WIDTH
@@ -230,48 +246,65 @@
     s = lax.broadcasted_iota(jnp.int32, (BLOCK, BLOCK), 1)
     causal = t >= s
     first_head = lax.broadcasted_iota(jnp.int32, (BLOCK, LANES), 1) < HEAD_DIM
+    started = jnp.zeros((1, running_ref.shape[1]), F32)
     for i in range(length // BLOCK):
         rows = slice(i * BLOCK, (i + 1) * BLOCK)
         running = running_ref[rows, :]
         padded = jnp.concatenate([running, jnp.zeros((BLOCK, BLOCK - running.shape[1]), F32)], axis=1)
         across = padded.T
+        since_block = jnp.exp(running)
+        since_start = jnp.exp(running + started)
+        started = started + running[BLOCK - 1 : BLOCK]
         for g in range(groups):
+            here = slice(g * width, (g + 1) * width)
             wide = slice(g * STATE_WIDTH, (g + 1) * STATE_WIDTH)
             products = dot(cc_ref[rows, wide], bc_ref[rows, wide], ((1,), (1,)))
             products = jnp.where(causal, products, 0.0)
+            gate = silu(gate_ref[rows, here].astype(F32))
+            factor_ref[rows, here] = (spread_heads(since_start, g, heads, width) * gate).astype(BF16)
+            carried = None
+            if i > 0:
+                read = dot(cc_ref[rows, wide], states_ref[i - 1, g].astype(BF16))
+                carried = read * spread_heads(since_block, g, heads, width)
             for p in range(width // LANES):
+                part = slice(p * LANES, (p + 1) * LANES)
                 cols = slice(g * width + p * LANES, g * width + (p + 1) * LANES)
                 pair = xdt_ref[rows, cols]
                 total = direct_ref[:, cols] * xc_ref[rows, cols].astype(F32)
+                if carried is not None:
+                    total = total + carried[:, part]
                 for q in range(LANES // HEAD_DIM):
                     h = g * heads + p * (LANES // HEAD_DIM) + q
                     spread = running[:, h : h + 1] - across[h : h + 1, :]
                     weights = (products * jnp.exp(jnp.where(causal, spread, 0.0))).astype(BF16)
                     keep = first_head if q == 0 else ~first_head
                     total = total + dot(weights, jnp.where(keep, pair, jnp.zeros_like(pair)))
-                y_ref[rows, cols] = total
-
-
-def local_outputs(c, tail, cf, bc, xdt, xc, running, direct):
+                fixed_ref[rows, cols] = (total * gate[:, part]).astype(BF16)
+
+
+def local_outputs(c, tail, cf, bc, xdt, xc, running, states, direct, gate):
     length, channels = xdt.shape
     return pl.pallas_call(
         local_kernel,
-        out_shape=(pltpu.HBM(c.shape, BF16), pltpu.HBM((length, channels), F32)),
-        in_specs=[VMEM] * 8,
-        out_specs=(VMEM, VMEM),
+        out_shape=(
+            near(c.shape, BF16),
+            near((length, channels), BF16),
+            near((length, channels), BF16),
+        ),
+        in_specs=[VMEM] * 10,
+        out_specs=(VMEM,) * 3,
         scratch_shapes=[pltpu.VMEM((8 + length, LANES), F32)],
-        compiler_params=limit(12),
+        compiler_params=limit(14),
         name="local_outputs",
-    )(c, tail, cf, bc, xdt, xc, running, direct)
-
-
-def project_kernel(y_ref, cc_ref, states_ref, incoming_ref, running_ref, gate_ref, scale_ref, w_hbm, out_ref, w_ref, rows_ref, sem):
+    )(c, tail, cf, bc, xdt, xc, running, states, direct, gate)
+
+
+def project_kernel(fixed_ref, factor_ref, cc_ref, incoming_ref, scale_ref, w_hbm, out_ref, w_ref, rows_ref, sem):
     copy = pltpu.make_async_copy(w_hbm, w_ref, sem)
     copy.start()
-    length, channels = y_ref.shape
+    length, channels = fixed_ref.shape
     groups = cc_ref.shape[1] // STATE_WIDTH
     width = channels // groups
-    heads = width // HEAD_DIM
     tiles = width // LANES
     for g in range(groups):
         here = slice(g * width, (g + 1) * width)
@@ -280,18 +313,11 @@
         for n in range(STATE_WIDTH // 16):
             at = (g * (STATE_WIDTH // 16) + n) * tiles
             lines.append(jnp.concatenate([incoming_ref[at + p] for p in range(tiles)], axis=1))
-        incoming = jnp.concatenate(lines, axis=0).astype(F32)
-        started = jnp.zeros((1, running_ref.shape[1]), F32)
+        incoming = jnp.concatenate(lines, axis=0)
         for i in range(length // BLOCK):
             rows = slice(i * BLOCK, (i + 1) * BLOCK)
-            running = running_ref[rows, :]
-            if i == 0:
-                state = incoming
-            else:
-                state = states_ref[i - 1, g] + incoming * spread_heads(jnp.exp(started), g, heads, width)
-            started = started + running[BLOCK - 1 : BLOCK]
-            read = dot(cc_ref[rows, wide], state.astype(BF16)) * spread_heads(jnp.exp(running), g, heads, width)
-            gated = (y_ref[rows, here] + read) * silu(gate_ref[rows, here].astype(F32))
+            read = dot(cc_ref[rows, wide], incoming)
+            gated = fixed_ref[rows, here].astype(F32) + read * factor_ref[rows, here].astype(F32)
             power = jnp.mean(gated * gated, axis=1, keepdims=True)
             normed = gated * lax.rsqrt(power + EPS) * scale_ref[:, here].astype(F32)
             rows_ref[rows, here] = normed.astype(BF16)
@@ -299,12 +325,12 @@
     out_ref[...] = dot(rows_ref[...], w_ref[...]).astype(BF16)
 
 
-def projected(y, cc, states, incoming, running, gate, scale, w):
-    length, channels = y.shape
+def projected(fixed, factor, cc, incoming, scale, w):
+    length, channels = fixed.shape
     return pl.pallas_call(
         project_kernel,
-        out_shape=shape_of((length, w.shape[1]), BF16),
-        in_specs=[VMEM] * 7 + [ANY],
+        out_shape=near((length, w.shape[1]), BF16),
+        in_specs=[VMEM] * 5 + [ANY],
         out_specs=VMEM,
         scratch_shapes=[
             pltpu.VMEM(w.shape, BF16),
@@ -313,7 +339,7 @@
         ],
         compiler_params=limit(20),
         name="projected",
-    )(y, cc, states, held(incoming), running, gate, scale, *far_off(w))
+    )(held(fixed), held(factor), held(cc), held(incoming), scale, *far_off(w))
 
 
 def slots_kernel(capacity, routes_ref, slots_ref, count_ref):
@@ -393,25 +419,23 @@
     )(held(parts), residual, gain, bias, slots)
 
 
-def expert_kernel(arrived_ref, *refs):
+def expert_kernel(places, arrived_ref, *refs):
     pieces = refs[:-6]
     out_ref, blocks_ref, x_ref, hidden_ref, buffer_ref, sem = refs[-6:]
     slots, chunks, _ = arrived_ref.shape
     width = chunks * LANES
     quarters, _, units = buffer_ref.shape
     copies = []
-    for n, source in enumerate(pieces):
-        size = source.shape[0]
-        own = n < 3
-        quarter = 0 if own else 1 + (n - 3) // 2
-        start = n * width if own else (n - 3) % 2 * size
-        copies.append((quarter, pltpu.make_async_copy(source, buffer_ref.at[quarter, pl.ds(start, size)], sem.at[n])))
+    for n, (which, at, size, quarter, to) in enumerate(places):
+        source = pieces[which].at[pl.ds(at, size)]
+        copies.append((quarter, pltpu.make_async_copy(source, buffer_ref.at[quarter, pl.ds(to, size)], sem.at[n])))
     for _, copy in copies:
         copy.start()
     for s in range(0, slots, 16):
-        blocks_ref[s * chunks : (s + 16) * chunks, :] = arrived_ref[s : s + 16].reshape(16 * chunks, LANES).astype(F32)
+        for r in range(s, s + 16):
+            blocks_ref[r * PITCH : r * PITCH + chunks, :] = arrived_ref[r].astype(F32)
     for c in range(chunks):
-        x_ref[:, c * LANES : (c + 1) * LANES] = blocks_ref[pl.ds(c, slots, stride=chunks), :].astype(BF16)
+        x_ref[:, c * LANES : (c + 1) * LANES] = blocks_ref[pl.ds(c, slots, stride=PITCH), :].astype(BF16)
     for q in range(quarters):
         for quarter, copy in copies:
             if quarter == q:
@@ -427,49 +451,79 @@
             part = dot(hidden_ref[:, q * units : (q + 1) * units], down, ((1,), (1,)))
             total = part if total is None else total + part
         for c in range(step // LANES):
-            blocks_ref[pl.ds(n // LANES + c, slots, stride=chunks), :] = total[:, c * LANES : (c + 1) * LANES]
+            blocks_ref[pl.ds(n // LANES + c, slots, stride=PITCH), :] = total[:, c * LANES : (c + 1) * LANES]
     for s in range(0, slots, 16):
-        out_ref[s : s + 16] = blocks_ref[s * chunks : (s + 16) * chunks, :].astype(BF16).reshape(16, chunks, LANES)
-
-
-def expert_answers(arrived, own, packs):
+        for r in range(s, s + 16):
+            out_ref[r] = blocks_ref[r * PITCH : r * PITCH + chunks, :].astype(BF16)
+
+
+def expert_answers(arrived, pieces, places):
     slots, chunks, _ = arrived.shape
     width = chunks * LANES
-    units = own[0].shape[1]
-    pieces = [*own, *packs]
-    return pl.pallas_call(
-        expert_kernel,
+    units = pieces[0].shape[1]
+    return pl.pallas_call(
+        lambda *refs: expert_kernel(places, *refs),
         out_shape=shape_of(arrived.shape, BF16),
         in_specs=[VMEM] + [ANY] * len(pieces),
         out_specs=VMEM,
         scratch_shapes=[
-            pltpu.VMEM((slots * chunks, LANES), F32),
+            pltpu.VMEM((slots * PITCH, LANES), F32),
             pltpu.VMEM((slots, width), BF16),
             pltpu.VMEM((slots, 4 * units), BF16),
             pltpu.VMEM((4, 3 * width, units), BF16),
-            pltpu.SemaphoreType.DMA((len(pieces),)),
+            pltpu.SemaphoreType.DMA((len(places),)),
         ],
         compiler_params=limit(36),
         name="expert_answers",
     )(held(arrived), *far_off(*pieces))
 
 
-def pack_kernel(gate_ref, up_ref, down_ref, first_ref, second_ref, stage_ref, into, out):
-    width = gate_ref.shape[0]
-    half = width // 2
-    sources = (
-        gate_ref.at[pl.ds(0, half)],
-        gate_ref.at[pl.ds(half, half)],
-        up_ref.at[pl.ds(0, half)],
-        up_ref.at[pl.ds(half, half)],
-        down_ref.at[pl.ds(0, half)],
-        down_ref.at[pl.ds(half, half)],
-    )
-    loads = [pltpu.make_async_copy(source, stage_ref.at[n], into.at[n]) for n, source in enumerate(sources)]
-    stores = []
-    for n in range(len(sources)):
-        target = first_ref if n < 3 else second_ref
-        stores.append(pltpu.make_async_copy(stage_ref.at[n], target.at[pl.ds(n % 3 * half, half)], out.at[n]))
+def enter_kernel(*refs):
+    count = (len(refs) - 1) // 2
+    sources, tail_ref, targets, sem = refs[:count], refs[count], refs[count + 1 : -1], refs[-1]
+    rows = tail_ref.shape[0]
+    copies = []
+    start = 0
+    for n, ref in enumerate((sources[0], sources[1], sources[-1])):
+        length, width = ref.shape
+        source = ref.at[pl.ds(length - rows, rows)]
+        copies.append(pltpu.make_async_copy(source, tail_ref.at[:, pl.ds(start, width)], sem.at[n]))
+        start += width
+    for n, (source, target) in enumerate(zip(sources[:-1], targets)):
+        copies.append(pltpu.make_async_copy(source, target, sem.at[3 + n]))
+    for copy in copies:
+        copy.start()
+    for copy in copies:
+        copy.wait()
+
+
+def entered(rows, values, last):
+    width = values[0].shape[1] + values[1].shape[1] + last.shape[1]
+    count = len(values)
+    return pl.pallas_call(
+        enter_kernel,
+        out_shape=(near((rows, width), BF16), *(near(value.shape, value.dtype) for value in values)),
+        in_specs=[ANY] * (count + 1),
+        out_specs=(VMEM,) * (count + 1),
+        scratch_shapes=[pltpu.SemaphoreType.DMA((3 + count,))],
+        compiler_params=limit(1),
+        name="entered",
+    )(*far_off(*values, last))
+
+
+def moved_kernel(moves, *refs):
+    count = len(refs) - 5
+    sources, targets, stage_ref, into, out = refs[:count], refs[count : count + 2], refs[-3], refs[-2], refs[-1]
+    step = stage_ref.shape[1]
+    loads, stores = [], []
+    for target, parts in zip(targets, moves):
+        to = 0
+        for which, start, size in parts:
+            for at in range(start, start + size, step):
+                n = len(loads)
+                loads.append(pltpu.make_async_copy(sources[which].at[pl.ds(at, step)], stage_ref.at[n], into.at[n]))
+                stores.append(pltpu.make_async_copy(stage_ref.at[n], target.at[pl.ds(to, step)], out.at[n]))
+                to += step
     for load in loads:
         load.start()
     for load, store in zip(loads, stores):
@@ -479,49 +533,24 @@
         store.wait()
 
 
-def packed(gate, up, down):
-    width, units = gate.shape
-    both = pltpu.HBM((width * 3 // 2, units), BF16)
-    return pl.pallas_call(
-        pack_kernel,
-        out_shape=(both, both),
-        in_specs=[ANY] * 3,
-        out_specs=(ANY, ANY),
+def moved(values, *moves):
+    units = values[0].shape[1]
+    step = min(size for parts in moves for _, _, size in parts) // 2
+    rows = [sum(size for _, _, size in parts) for parts in moves]
+    count = sum(rows) // step
+    return pl.pallas_call(
+        lambda *refs: moved_kernel(moves, *refs),
+        out_shape=tuple(pltpu.HBM((size, units), BF16) for size in rows),
+        in_specs=[ANY] * len(values),
+        out_specs=(ANY,) * len(moves),
         scratch_shapes=[
-            pltpu.VMEM((6, width // 2, units), BF16),
-            pltpu.SemaphoreType.DMA((6,)),
-            pltpu.SemaphoreType.DMA((6,)),
+            pltpu.VMEM((count, step, units), BF16),
+            pltpu.SemaphoreType.DMA((count,)),
+            pltpu.SemaphoreType.DMA((count,)),
         ],
-        compiler_params=limit(8),
-        name="packed",
-    )(*far_off(gate, up, down))
-
-
-def tail_kernel(x_ref, b_ref, c_ref, out_ref, sem):
-    rows = out_ref.shape[0]
-    copies = []
-    start = 0
-    for n, ref in enumerate((x_ref, b_ref, c_ref)):
-        length, width = ref.shape
-        source = ref.at[pl.ds(length - rows, rows)]
-        copies.append(pltpu.make_async_copy(source, out_ref.at[:, pl.ds(start, width)], sem.at[n]))
-        start += width
-    for copy in copies:
-        copy.start()
-    for copy in copies:
-        copy.wait()
-
-
-def last_rows(x, b, c, rows):
-    return pl.pallas_call(
-        tail_kernel,
-        out_shape=near((rows, x.shape[1] + b.shape[1] + c.shape[1]), BF16),
-        in_specs=[ANY] * 3,
-        out_specs=VMEM,
-        scratch_shapes=[pltpu.SemaphoreType.DMA((3,))],
-        compiler_params=limit(1),
-        name="last_rows",
-    )(*far_off(x, b, c))
+        compiler_params=limit(12),
+        name="moved",
+    )(*far_off(*values))
 
 
 def final_kernel(top_count, returned_ref, middle_ref, slots_ref, weights_ref, gain_ref, bias_ref, out_ref, blocks_ref):
@@ -598,37 +627,58 @@
     capacity = 5
 
     own = (expert_gate_weight[0], expert_up_weight[0], expert_down_weight[0])
-    ending = last_rows(head_input_values, group_input_vectors, group_readout_vectors, 8)
+    ending, *entering = entered(
+        8,
+        (
+            head_input_values,
+            group_input_vectors,
+            head_input_filter,
+            input_vector_filter,
+            step_size_logits.T,
+            extra_log_decay.T,
+            step_size_bias[None],
+            head_rate_logarithm[None],
+        ),
+        group_readout_vectors,
+    )
     tail = lax.ppermute(ending, SP, [(i, i + 1) for i in range(devices - 1)])
-    first, second = packed(*own)
-    first_behind = turned_by(first, 1)
-    first_ahead = turned_by(first, -1)
-    second_behind = turned_by(second, 1)
-    second_ahead = turned_by(second, -1)
-    xc, xdt, bc, running, states, message = end_states(
-        head_input_values,
-        group_input_vectors,
-        tail,
-        head_input_filter,
-        input_vector_filter,
-        step_size_logits.T,
-        extra_log_decay.T,
-        step_size_bias[None],
-        head_rate_logarithm[None],
-    )
+    gate, up, down = own
+    up_behind = turned_by(up, 1)
+    up_ahead = turned_by(up, -1)
+    gate_behind = turned_by(gate, 1)
+    down_ahead = turned_by(down, -1)
+    xc, xdt, bc, running, states, message = end_states(tail, *entering)
     met = exchanged(message, SP)
     slots = slot_layout(routes.T, capacity, experts)
     direct = jnp.repeat(direct_path_weight, HEAD_DIM)[None]
-    cc, y = local_outputs(group_readout_vectors, tail, readout_vector_filter, bc, xdt, xc, running, direct)
+    cc, fixed, factor = local_outputs(
+        group_readout_vectors,
+        tail,
+        readout_vector_filter,
+        bc,
+        xdt,
+        xc,
+        running,
+        states,
+        direct,
+        output_gate_values,
+    )
     incoming = exchanged(chain(met), SP)
-    sums = projected(
-        y, cc, states, incoming, running, output_gate_values, group_norm_scale[None], mixer_output_weight
-    )
+    half = width // 2
+    low, high = moved((up_behind, up_ahead), ((0, 0, half),), ((1, half, half),))
+    up_low = turned_by(low, 1)
+    up_high = turned_by(high, -1)
+    sums = projected(fixed, factor, cc, incoming, group_norm_scale[None], mixer_output_weight)
     peers = lax.axis_size("tp")
     parts = exchanged(sums.reshape(peers, rows_here, width), "tp")
-    first_behind, second_ahead, parts = lax.optimization_barrier((first_behind, second_ahead, parts))
-    first_far = turned_by(first_behind, 1)
-    second_far = turned_by(second_ahead, -1)
+    onward = moved(
+        (gate_behind, down, down_ahead, gate),
+        ((0, 0, width), (1, 0, width)),
+        ((2, 0, width), (3, 0, width)),
+    )
+    onward, parts = lax.optimization_barrier((onward, parts))
+    last_on = turned_by(onward[0], 1)
+    last_back = turned_by(onward[1], -1)
     middle, outgoing = middle_rows(
         parts, residual, first_norm_scale[None], first_norm_bias[None], slots, top_count, experts * capacity
     )
@@ -636,8 +686,22 @@
     arrived = exchanged(outgoing.reshape(experts, capacity * chunks, LANES), SP)
     answers = expert_answers(
         arrived.reshape(experts * capacity, chunks, LANES),
-        own,
-        (first_behind, second_behind, first_ahead, second_ahead, first_far, second_far),
+        (gate, up, down, gate_behind, up_behind, up_ahead, down_ahead, up_low, up_high, last_on, last_back),
+        (
+            (0, 0, width, 0, 0),
+            (1, 0, width, 0, width),
+            (2, 0, width, 0, 2 * width),
+            (3, 0, width, 1, 0),
+            (4, 0, width, 1, width),
+            (9, width, width, 1, 2 * width),
+            (10, width, width, 2, 0),
+            (5, 0, width, 2, width),
+            (6, 0, width, 2, 2 * width),
+            (9, 0, width, 3, 0),
+            (7, 0, half, 3, width),
+            (8, 0, half, 3, width + half),
+            (10, 0, width, 3, 2 * width),
+        ),
     )
     returned = exchanged(answers.reshape(experts, capacity * chunks, LANES), SP)
     return final_rows(

time: 252 us -> 273 us (1.083)
  waiting for transfers between devices: 103 us -> 123 us
    ppermute x6 -> x8, waiting for transfers between devices: 81.9 us -> 114 us  [turned_by(): lax.ppermute(value, 'tp', [(i, (i + distance) % peers) for i in range(pee...]
    all_to_all x3, waiting for transfers between devices: 18.2 us -> 5.69 us  [exchanged(): return lax.all_to_all(value, axis, split_axis=0, concat_axis=0, tiled=True)]
    all_to_all x3, starting transfers between devices: 20.8 us -> 16 us  [exchanged(): return lax.all_to_all(value, axis, split_axis=0, concat_axis=0, tiled=True)]
    ppermute x6 -> x8, starting transfers between devices: 8.65 us -> 13.1 us  [turned_by(): lax.ppermute(value, 'tp', [(i, (i + distance) % peers) for i in range(pee...]
    pallas_call x5 -> x6, Pallas kernels: 21 us -> 21.8 us  [the longest x1 6.98 us: expert_answers(): pl.pallas_call(lambda *refs: expert_kernel(places, *refs), out_shape=shap...]
    unnamed x62 -> x56, local copies, waits for them, and re-layouts: 9.86 us -> 10.7 us
  transfers between devices with their start and end apart: 10 -> 12, of which waited for: 8 -> 5; matrix products, arithmetic and copies ran while one was open for 0% -> 0% of each run, Pallas kernels for 6% -> 4%
where the time goes in v2:
time: 273 us; the launch traced here: 272 us
  waiting for transfers between devices  123 us (45%)
  blocking collectives  72.1 us (26%)
  Pallas kernels  34.3 us (13%)
  starting transfers between devices  31.1 us (11%)
  local copies, waits for them, and re-layouts  10.9 us (4%)
    ppermute x8, waiting for transfers between devices, turned_by(): lax.ppermute(value, 'tp', [(i, (i + distance) % peers) for i in range(pee...  114 us
    all_to_all x2, blocking collectives, exchanged(): return lax.all_to_all(value, axis, split_axis=0, concat_axis=0, tiled=True)  72.1 us
    all_to_all x3, starting transfers between devices, exchanged(): return lax.all_to_all(value, axis, split_axis=0, concat_axis=0, tiled=True)  16 us
    ppermute x8, starting transfers between devices, turned_by(): lax.ppermute(value, 'tp', [(i, (i + distance) % peers) for i in range(pee...  13.1 us
    unnamed x56, local copies, waits for them, and re-layouts  10.7 us
    pallas_call x1, Pallas kernels, expert_answers(): pl.pallas_call(lambda *refs: expert_kernel(places, *refs), out_shape=shap...  6.98 us
    pallas_call x1, Pallas kernels, projected(): pl.pallas_call(project_kernel, out_shape=near((length, w.shape[1]), BF16)...  5.71 us
    all_to_all x3, waiting for transfers between devices, exchanged(): return lax.all_to_all(value, axis, split_axis=0, concat_axis=0, tiled=True)  5.69 us
  transfers between devices with their start and end apart: 12, of which 5 were waited for; matrix products, arithmetic and copies ran while one was open for 0% of the time, Pallas kernels for 4%

profile of v2, /device:TPU:8, one launch (start us, length us, event | category | flops | bytes accessed | tf_op | source)
XLA Modules:
  0.0 271.8 jit_solution(13237348650938224901)
XLA Ops:
  1.4 2.1 collective-permute-start.2
  3.4 3.2 %collective-permute-done.2.tail_ref = bf16[8,1536]{1,0:T(8,128)(2,1)S(1)} collective-permute-done((bf16[8,1536]{1,0:T(8,128)(2,1)S(1)}, bf16[8,1536]{1,0:T(8,128)(2,1)S(1)}, u32[]{:S(2)}, u32[]{:S(2)}) %collective-permute-start.2) | collective-permute-done | bytes 24608 | tf_op jit(solution)/shard_map/ppermute | solution.py:644
  6.7 4.3 %end_states.1 = (bf16[384,1024]{1,0:T(8,128)(2,1)}, bf16[384,1024]{1,0:T(8,128)(2,1)}, bf16[384,256]{1,0:T(8,128)(2,1)}, f32[384,16]{1,0:T(8,128)}, f32[2,2,128,...) custom-call(bf16[384,1024]{1,0:T(8,128)(2,1)S(1)} %get-tuple-element.35.x_ref, ...), custom_call_target="tpu_custom_call" | custom-call | tf_op jit(solution)/shard_map/end_states/pallas_call | solution.py:178
  10.9 27.4 %all_to_all.25.parts_ref = bf16[64,24,128]{2,1,0:T(8,128)(2,1)S(1)} all-to-all(bf16[64,24,128]{2,1,0:T(8,128)(2,1)S(1)} %get-tuple-element.51), channel_id=1, replica_groups=mesh['sp'=64,'tp'=4] {'sp'}, dimensions={0} | all-to-all | bytes 786432 | tf_op jit(solution)/shard_map/all_to_all | solution.py:594
  39.3 5.9 %all-to-all-start.1 = ((bf16[64,16,128]{2,1,0:T(8,128)(2,1)}), bf16[64,16,128]{2,1,0:T(8,128)(2,1)S(1)}, u32[]{:S(2)}, u32[]{:S(2)}) async-start(bf16[64,16,128]{2,1,0:T(8,128)(2,1)} %chain.1), calls=%async_computation.1 | async-start | bytes 524288 | tf_op jit(solution)/shard_map/all_to_all | solution.py:594
  48.9 2.2 local_outputs.1
  51.7 5.7 %all-to-all-done.1.incoming_ref = bf16[64,16,128]{2,1,0:T(8,128)(2,1)S(1)} async-done(((bf16[64,16,128]{2,1,0:T(8,128)(2,1)}), bf16[64,16,128]{2,1,0:T(8,128)(2,1)S(1)}, u32[]{:S(2)}, u32[]{:S(2)}) %all-to-all-start.1) | async-done | bytes 262176 | tf_op jit(solution)/shard_map/all_to_all | solution.py:594
  58.4 5.7 %projected.1 = bf16[384,2048]{1,0:T(8,128)(2,1)} custom-call(bf16[384,1024]{1,0:T(8,128)(2,1)S(1)} %get-tuple-element.48.fixed_ref, bf16[384,1024]{1,0:T(8,128)(2,1)S(1)} %get-tuple-element.49.factor_ref, bf16[384,256]{1,0:T(8,128)(2,1)S(1)} %copy-done.9, bf16[64,16,128]{2,1,0:T(8,128)(2,1)S(1)} %all-to-all-done.1.incoming_ref, ...), custom_call_target="tpu_custom_call" | custom-call | tf_op jit(solution)/shard_map/projected/pallas_call | solution.py:330
  64.1 4.4 %all-to-all-start.2 = ((bf16[4,96,2048]{2,1,0:T(8,128)(2,1)}), bf16[4,96,2048]{2,1,0:T(8,128)(2,1)S(1)}, u32[]{:S(2)}, u32[]{:S(2)}) async-start(bf16[4,96,2048]{2,1,0:T(8,128)(2,1)} %bitcast.6), calls=%async_computation.2 | async-start | bytes 3145728 | tf_op jit(solution)/shard_map/all_to_all | solution.py:594
  68.5 2.0 collective-permute-start
  71.8 2.2 slot_layout.1.refs_4_.refs_2_
  74.0 37.7 %collective-permute-done.refs_0_.refs_4_ = bf16[2048,256]{1,0:T(8,128)(2,1)S(1)} collective-permute-done((bf16[2048,256]{1,0:T(8,128)(2,1)S(1)}, bf16[2048,256]{1,0:T(8,128)(2,1)S(1)}, u32[]{:S(2)}, u32[]{:S(2)}) %collective-permute-start) | collective-permute-done | bytes 1048608 | tf_op jit(solution)/shard_map/ppermute | solution.py:590
  113.8 3.6 %moved.2 = (bf16[4096,256]{1,0:T(8,128)(2,1)}, bf16[4096,256]{1,0:T(8,128)(2,1)}) custom-call(bf16[2048,256]{1,0:T(8,128)(2,1)} %copy-done.20, bf16[2048,256]{1,0:T(8,128)(2,1)} %bitcast.31, bf16[2048,256]{1,0:T(8,128)(2,1)} %copy-done.21, bf16[2048,256]{1,0:T(8,128)(2,1)} %bitcast.27), custom_call_target="tpu_custom_call" | custom-call | tf_op jit(solution)/shard_map/moved/pallas_call | solution.py:541
  117.4 2.7 middle_rows.1
  120.1 5.7 %all-to-all-start.3 = ((bf16[64,80,128]{2,1,0:T(8,128)(2,1)}), bf16[64,80,128]{2,1,0:T(8,128)(2,1)S(1)}, u32[]{:S(2)}, u32[]{:S(2)}) async-start(bf16[64,80,128]{2,1,0:T(8,128)(2,1)} %bitcast.10), calls=%async_computation.3 | async-start | bytes 2621440 | tf_op jit(solution)/shard_map/all_to_all | solution.py:594
  125.9 3.2 %collective-permute-start.8 = (bf16[4096,256]{1,0:T(8,128)(2,1)}, bf16[4096,256]{1,0:T(8,128)(2,1)}, u32[]{:S(2)}, u32[]{:S(2)}) collective-permute-start(bf16[4096,256]{1,0:T(8,128)(2,1)} %get-tuple-element.57), channel_id=1, source_target_pairs={{0,3},{1,0},{2,1},{3,2},{4,7},{5,4},{6,5},{7,6},{8,11},{9,8},{10,9... | collective-permute-start | bytes 6291464 | tf_op jit(solution)/shard_map/ppermute | solution.py:590
  129.1 3.2 %collective-permute-start.4 = (bf16[2048,256]{1,0:T(8,128)(2,1)S(1)}, bf16[2048,256]{1,0:T(8,128)(2,1)S(1)}, u32[]{:S(2)}, u32[]{:S(2)}) collective-permute-start(bf16[2048,256]{1,0:T(8,128)(2,1)S(1)} %bitcast.35), channel_id=1, source_target_pairs={{0,3},{1,0},{2,1},{3,2},{4,7},{5,4},{6,5},{7,6},{8,11},{9,8},{10,9... | collective-permute-start | bytes 3145736 | tf_op jit(solution)/shard_map/ppermute | solution.py:590
  132.3 65.1 %collective-permute-done.3.refs_0_.refs_5_ = bf16[2048,256]{1,0:T(8,128)(2,1)S(1)} collective-permute-done((bf16[2048,256]{1,0:T(8,128)(2,1)S(1)}, bf16[2048,256]{1,0:T(8,128)(2,1)S(1)}, u32[]{:S(2)}, u32[]{:S(2)}) %collective-permute-start.3) | collective-permute-done | bytes 1048608 | tf_op jit(solution)/shard_map/ppermute | solution.py:590
  199.4 2.0 moved.3
  201.5 3.2 %collective-permute-start.6 = (bf16[1024,256]{1,0:T(8,128)(2,1)}, bf16[1024,256]{1,0:T(8,128)(2,1)S(1)}, u32[]{:S(2)}, u32[]{:S(2)}) collective-permute-start(bf16[1024,256]{1,0:T(8,128)(2,1)} %get-tuple-element.55), channel_id=1, source_target_pairs={{0,3},{1,0},{2,1},{3,2},{4,7},{5,4},{6,5},{7,6},{8,11},{9,8},{10,9... | collective-permute-start | bytes 1572872 | tf_op jit(solution)/shard_map/ppermute | solution.py:590
  204.7 11.3 %collective-permute-done.5.refs_8_ = bf16[1024,256]{1,0:T(8,128)(2,1)S(1)} collective-permute-done((bf16[1024,256]{1,0:T(8,128)(2,1)}, bf16[1024,256]{1,0:T(8,128)(2,1)S(1)}, u32[]{:S(2)}, u32[]{:S(2)}) %collective-permute-start.5) | collective-permute-done | bytes 524320 | tf_op jit(solution)/shard_map/ppermute | solution.py:590
  217.7 7.0 %expert_answers.1 = bf16[320,16,128]{2,1,0:T(8,128)(2,1)S(1)} custom-call(bf16[320,16,128]{2,1,0:T(8,128)(2,1)S(1)} %bitcast.19, bf16[2048,256]{1,0:T(8,128)(2,1)} %bitcast.28, bf16[2048,256]{1,0:T(8,128)(2,1)} %bitcast.33, bf16[2048,256]{1,0:T(8,128)(2,1)} %bitcast.32, bf16[2048,256]{1,0:T(8,128)(2,1)} %copy-done.20, bf16[2048,256]{1,0:T(8,128)(2,1)} %copy-done.17, ...), custom_call_target="tpu_custom_call" | custom-call | tf_op jit(solution)/shard_map/expert_answers/pallas_call | solution.py:464
  224.7 44.7 %all_to_all.26 = bf16[64,80,128]{2,1,0:T(8,128)(2,1)S(1)} all-to-all(bf16[64,80,128]{2,1,0:T(8,128)(2,1)S(1)} %bitcast.20), channel_id=1, replica_groups=mesh['sp'=64,'tp'=4] {'sp'}, dimensions={0} | all-to-all | bytes 2621440 | tf_op jit(solution)/shard_map/all_to_all | solution.py:594
  269.4 2.3 final_rows.1
  (72 shorter events, 14.6 us)
Async XLA Ops:
  1.3 43.9 %copy-start.27 = (f32[16]{0:T(128)S(1)}, f32[16]{0:T(128)}, u32[]{:S(2)}) copy-start(f32[16]{0:T(128)} %param.35) | copy-start | bytes 196
  1.3 44.1 %copy-start.26 = (bf16[1024]{0:T(1024)(128)(2,1)S(1)}, bf16[1024]{0:T(1024)(128)(2,1)}, u32[]{:S(2)}) copy-start(bf16[1024]{0:T(1024)(128)(2,1)} %param.36) | copy-start | bytes 6148
  1.4 44.1 %copy-start.1 = (bf16[384,256]{1,0:T(8,128)(2,1)S(1)}, bf16[384,256]{1,0:T(8,128)(2,1)}, u32[]{:S(2)}) copy-start(bf16[384,256]{1,0:T(8,128)(2,1)} %c_ref.1) | copy-start | bytes 589828
  1.4 44.1 %copy-start.14 = (bf16[4,256]{1,0:T(4,128)(2,1)S(1)}, bf16[4,256]{1,0:T(4,128)(2,1)}, u32[]{:S(2)}) copy-start(bf16[4,256]{1,0:T(4,128)(2,1)} %cf_ref.1) | copy-start | bytes 6148
  1.4 5.3 %collective-permute-start.2 = (bf16[8,1536]{1,0:T(8,128)(2,1)S(1)}, bf16[8,1536]{1,0:T(8,128)(2,1)S(1)}, u32[]{:S(2)}, u32[]{:S(2)}) collective-permute-start(bf16[8,1536]{1,0:T(8,128)(2,1)S(1)} %get-tuple-element.34), channel_id=1, source_target_pairs={{0,4},{4,8},{8,12},{12,16},{16,20},{20,24},{24,28},{28,32},{32,36}... | collective-permute-start | bytes 73736 | tf_op jit(solution)/shard_map/ppermute | solution.py:644
  10.9 34.5 %copy-start.6 = (bf16[384,256]{1,0:T(8,128)(2,1)S(1)}, bf16[384,256]{1,0:T(8,128)(2,1)}, u32[]{:S(2)}) copy-start(bf16[384,256]{1,0:T(8,128)(2,1)} %get-tuple-element.43.bc_ref) | copy-start | bytes 589828
  10.9 34.5 %copy-start.7 = (f32[384,16]{1,0:T(8,128)S(1)}, f32[384,16]{1,0:T(8,128)}, u32[]{:S(2)}) copy-start(f32[384,16]{1,0:T(8,128)} %get-tuple-element.46.running_ref) | copy-start | bytes 73732
  39.3 18.1 %all-to-all-start.1 = ((bf16[64,16,128]{2,1,0:T(8,128)(2,1)}), bf16[64,16,128]{2,1,0:T(8,128)(2,1)S(1)}, u32[]{:S(2)}, u32[]{:S(2)}) async-start(bf16[64,16,128]{2,1,0:T(8,128)(2,1)} %chain.1), calls=%async_computation.1 | async-start | bytes 524288 | tf_op jit(solution)/shard_map/all_to_all | solution.py:594
  64.1 53.3 %all-to-all-start.2 = ((bf16[4,96,2048]{2,1,0:T(8,128)(2,1)}), bf16[4,96,2048]{2,1,0:T(8,128)(2,1)S(1)}, u32[]{:S(2)}, u32[]{:S(2)}) async-start(bf16[4,96,2048]{2,1,0:T(8,128)(2,1)} %bitcast.6), calls=%async_computation.2 | async-start | bytes 3145728 | tf_op jit(solution)/shard_map/all_to_all | solution.py:594
  68.5 43.2 %collective-permute-start = (bf16[2048,256]{1,0:T(8,128)(2,1)S(1)}, bf16[2048,256]{1,0:T(8,128)(2,1)S(1)}, u32[]{:S(2)}, u32[]{:S(2)}) collective-permute-start(bf16[2048,256]{1,0:T(8,128)(2,1)S(1)} %bitcast.29), channel_id=1, source_target_pairs={{0,1},{1,2},{2,3},{3,0},{4,5},{5,6},{6,7},{7,4},{8,9},{9,10},{10,1... | collective-permute-start | bytes 3145736 | tf_op jit(solution)/shard_map/ppermute | solution.py:590
  70.6 41.2 %collective-permute-start.1 = (bf16[2048,256]{1,0:T(8,128)(2,1)}, bf16[2048,256]{1,0:T(8,128)(2,1)S(1)}, u32[]{:S(2)}, u32[]{:S(2)}) collective-permute-start(bf16[2048,256]{1,0:T(8,128)(2,1)} %bitcast.30), channel_id=1, source_target_pairs={{0,3},{1,0},{2,1},{3,2},{4,7},{5,4},{6,5},{7,6},{8,11},{9,8},{10,9... | collective-permute-start | bytes 3145736 | tf_op jit(solution)/shard_map/ppermute | solution.py:590
  74.0 43.4 %copy-start.5 = (bf16[96,2048]{1,0:T(8,128)(2,1)S(1)}, bf16[96,2048]{1,0:T(8,128)(2,1)}, u32[]{:S(2)}) copy-start(bf16[96,2048]{1,0:T(8,128)(2,1)} %refs_1_.3) | copy-start | bytes 1179652
  74.0 43.4 %copy-start.10 = (f32[2048]{0:T(1024)S(1)}, f32[2048]{0:T(1024)}, u32[]{:S(2)}) copy-start(f32[2048]{0:T(1024)} %param.39) | copy-start | bytes 24580
  74.0 43.4 %copy-start.11 = (f32[2048]{0:T(1024)S(1)}, f32[2048]{0:T(1024)}, u32[]{:S(2)}) copy-start(f32[2048]{0:T(1024)} %param.40) | copy-start | bytes 24580
  120.1 97.3 %all-to-all-start.3 = ((bf16[64,80,128]{2,1,0:T(8,128)(2,1)}), bf16[64,80,128]{2,1,0:T(8,128)(2,1)S(1)}, u32[]{:S(2)}, u32[]{:S(2)}) async-start(bf16[64,80,128]{2,1,0:T(8,128)(2,1)} %bitcast.10), calls=%async_computation.3 | async-start | bytes 2621440 | tf_op jit(solution)/shard_map/all_to_all | solution.py:594
  125.8 90.2 %collective-permute-start.7 = (bf16[4096,256]{1,0:T(8,128)(2,1)}, bf16[4096,256]{1,0:T(8,128)(2,1)S(1)}, u32[]{:S(2)}, u32[]{:S(2)}) collective-permute-start(bf16[4096,256]{1,0:T(8,128)(2,1)} %get-tuple-element.56), channel_id=1, source_target_pairs={{0,1},{1,2},{2,3},{3,0},{4,5},{5,6},{6,7},{7,4},{8,9},{9,10},{10,1... | collective-permute-start | bytes 6291464 | tf_op jit(solution)/shard_map/ppermute | solution.py:590
  125.9 91.5 %collective-permute-start.8 = (bf16[4096,256]{1,0:T(8,128)(2,1)}, bf16[4096,256]{1,0:T(8,128)(2,1)}, u32[]{:S(2)}, u32[]{:S(2)}) collective-permute-start(bf16[4096,256]{1,0:T(8,128)(2,1)} %get-tuple-element.57), channel_id=1, source_target_pairs={{0,3},{1,0},{2,1},{3,2},{4,7},{5,4},{6,5},{7,6},{8,11},{9,8},{10,9... | collective-permute-start | bytes 6291464 | tf_op jit(solution)/shard_map/ppermute | solution.py:590
  129.1 68.3 %collective-permute-start.3 = (bf16[2048,256]{1,0:T(8,128)(2,1)S(1)}, bf16[2048,256]{1,0:T(8,128)(2,1)S(1)}, u32[]{:S(2)}, u32[]{:S(2)}) collective-permute-start(bf16[2048,256]{1,0:T(8,128)(2,1)S(1)} %bitcast.34), channel_id=1, source_target_pairs={{0,1},{1,2},{2,3},{3,0},{4,5},{5,6},{6,7},{7,4},{8,9},{9,10},{10,1... | collective-permute-start | bytes 3145736 | tf_op jit(solution)/shard_map/ppermute | solution.py:590
  129.1 68.3 %collective-permute-start.4 = (bf16[2048,256]{1,0:T(8,128)(2,1)S(1)}, bf16[2048,256]{1,0:T(8,128)(2,1)S(1)}, u32[]{:S(2)}, u32[]{:S(2)}) collective-permute-start(bf16[2048,256]{1,0:T(8,128)(2,1)S(1)} %bitcast.35), channel_id=1, source_target_pairs={{0,3},{1,0},{2,1},{3,2},{4,7},{5,4},{6,5},{7,6},{8,11},{9,8},{10,9... | collective-permute-start | bytes 3145736 | tf_op jit(solution)/shard_map/ppermute | solution.py:590
  201.4 14.6 %collective-permute-start.5 = (bf16[1024,256]{1,0:T(8,128)(2,1)}, bf16[1024,256]{1,0:T(8,128)(2,1)S(1)}, u32[]{:S(2)}, u32[]{:S(2)}) collective-permute-start(bf16[1024,256]{1,0:T(8,128)(2,1)} %get-tuple-element.54), channel_id=1, source_target_pairs={{0,1},{1,2},{2,3},{3,0},{4,5},{5,6},{6,7},{7,4},{8,9},{9,10},{10,1... | collective-permute-start | bytes 1572872 | tf_op jit(solution)/shard_map/ppermute | solution.py:590
  201.5 14.5 %collective-permute-start.6 = (bf16[1024,256]{1,0:T(8,128)(2,1)}, bf16[1024,256]{1,0:T(8,128)(2,1)S(1)}, u32[]{:S(2)}, u32[]{:S(2)}) collective-permute-start(bf16[1024,256]{1,0:T(8,128)(2,1)} %get-tuple-element.55), channel_id=1, source_target_pairs={{0,3},{1,0},{2,1},{3,2},{4,7},{5,4},{6,5},{7,6},{8,11},{9,8},{10,9... | collective-permute-start | bytes 1572872 | tf_op jit(solution)/shard_map/ppermute | solution.py:590
  224.7 44.8 %copy-start.12 = (f32[2048]{0:T(1024)S(1)}, f32[2048]{0:T(1024)}, u32[]{:S(2)}) copy-start(f32[2048]{0:T(1024)} %param.46) | copy-start | bytes 24580
  224.7 44.7 %copy-start.13 = (f32[2048]{0:T(1024)S(1)}, f32[2048]{0:T(1024)}, u32[]{:S(2)}) copy-start(f32[2048]{0:T(1024)} %param.47) | copy-start | bytes 24580
  224.7 44.7 %copy-start.15 = (f32[96,2]{0,1:T(2,128)S(1)}, f32[96,2]{0,1:T(2,128)}, u32[]{:S(2)}) copy-start(f32[96,2]{0,1:T(2,128)} %param.42) | copy-start | bytes 2308
  (16 other events, 69.2 us)

commit v3 on v2

--- a/solution.py
+++ b/solution.py
@@ -299,9 +299,10 @@
     )(c, tail, cf, bc, xdt, xc, running, states, direct, gate)
 
 
-def project_kernel(fixed_ref, factor_ref, cc_ref, incoming_ref, scale_ref, w_hbm, out_ref, w_ref, rows_ref, sem):
-    copy = pltpu.make_async_copy(w_hbm, w_ref, sem)
-    copy.start()
+def project_kernel(fixed_ref, factor_ref, cc_ref, incoming_ref, scale_ref, w_hbm, out_ref, w_ref, rows_ref, read_ref, sem):
+    copies = [pltpu.make_async_copy(w_hbm.at[:, pl.ds(n * 512, 512)], w_ref.at[n], sem.at[n]) for n in range(4)]
+    for copy in copies:
+        copy.start()
     length, channels = fixed_ref.shape
     groups = cc_ref.shape[1] // STATE_WIDTH
     width = channels // groups
@@ -314,15 +315,18 @@
             at = (g * (STATE_WIDTH // 16) + n) * tiles
             lines.append(jnp.concatenate([incoming_ref[at + p] for p in range(tiles)], axis=1))
         incoming = jnp.concatenate(lines, axis=0)
-        for i in range(length // BLOCK):
-            rows = slice(i * BLOCK, (i + 1) * BLOCK)
-            read = dot(cc_ref[rows, wide], incoming)
-            gated = fixed_ref[rows, here].astype(F32) + read * factor_ref[rows, here].astype(F32)
+        read_ref[:, here] = dot(cc_ref[:, wide], incoming)
+    for g in range(groups):
+        here = slice(g * width, (g + 1) * width)
+        for i in range(0, length, 16):
+            rows = slice(i, i + 16)
+            gated = fixed_ref[rows, here].astype(F32) + read_ref[rows, here] * factor_ref[rows, here].astype(F32)
             power = jnp.mean(gated * gated, axis=1, keepdims=True)
             normed = gated * lax.rsqrt(power + EPS) * scale_ref[:, here].astype(F32)
             rows_ref[rows, here] = normed.astype(BF16)
-    copy.wait()
-    out_ref[...] = dot(rows_ref[...], w_ref[...]).astype(BF16)
+    for n, copy in enumerate(copies):
+        copy.wait()
+        out_ref[:, n * 512 : (n + 1) * 512] = dot(rows_ref[...], w_ref[n]).astype(BF16)
 
 
 def projected(fixed, factor, cc, incoming, scale, w):
@@ -333,9 +337,10 @@
         in_specs=[VMEM] * 5 + [ANY],
         out_specs=VMEM,
         scratch_shapes=[
-            pltpu.VMEM(w.shape, BF16),
+            pltpu.VMEM((4, w.shape[0], 512), BF16),
             pltpu.VMEM((length, channels), BF16),
-            pltpu.SemaphoreType.DMA,
+            pltpu.VMEM((length, channels), F32),
+            pltpu.SemaphoreType.DMA((4,)),
         ],
         compiler_params=limit(20),
         name="projected",
@@ -389,17 +394,17 @@
             mixed = mixed + parts_ref[k, rows, :].astype(F32)
         values = layer_norm(ALPHA * residual_ref[rows, :].astype(F32) + mixed, gain_ref[...], bias_ref[...])
         for c in range(chunks):
-            blocks_ref[pl.ds(r * chunks + c, 16, stride=chunks), :] = values[:, c * LANES : (c + 1) * LANES]
+            blocks_ref[pl.ds(r * PITCH + c, 16, stride=PITCH), :] = values[:, c * LANES : (c + 1) * LANES]
 
     def one(r, carry):
-        at = pl.multiple_of(r * chunks, 16)
+        at = pl.multiple_of(r * PITCH, 4)
         block = blocks_ref[pl.ds(at, chunks), :].astype(BF16)
         middle_ref[r] = block
         for k in range(top_count):
             out_ref[slots_ref[k, r]] = block
         return carry
 
-    lax.fori_loop(0, rows_here, one, 0, unroll=4)
+    lax.fori_loop(0, rows_here, one, 0, unroll=8)
 
 
 def middle_rows(parts, residual, gain, bias, slots, top_count, slot_total):
@@ -413,7 +418,7 @@
         ),
         in_specs=[VMEM] * 4 + [SMEM],
         out_specs=(VMEM, VMEM),
-        scratch_shapes=[pltpu.VMEM((rows_here * chunks, LANES), F32)],
+        scratch_shapes=[pltpu.VMEM((rows_here * PITCH, LANES), F32)],
         compiler_params=limit(8),
         name="middle_rows",
     )(held(parts), residual, gain, bias, slots)
@@ -560,14 +565,14 @@
         total = returned_ref[slots_ref[0, r]].astype(F32) * weights_ref[0, r]
         for k in range(1, top_count):
             total = total + returned_ref[slots_ref[k, r]].astype(F32) * weights_ref[k, r]
-        start = pl.multiple_of(r * chunks, 16)
+        start = pl.multiple_of(r * PITCH, 4)
         blocks_ref[pl.ds(start, chunks), :] = ALPHA * middle_ref[r].astype(F32) + total
         return carry
 
-    lax.fori_loop(0, rows_here, one, 0, unroll=4)
+    lax.fori_loop(0, rows_here, one, 0, unroll=8)
     for r in range(0, rows_here, 16):
         values = jnp.concatenate(
-            [blocks_ref[pl.ds(r * chunks + c, 16, stride=chunks), :] for c in range(chunks)], axis=1
+            [blocks_ref[pl.ds(r * PITCH + c, 16, stride=PITCH), :] for c in range(chunks)], axis=1
         )
         out_ref[r : r + 16, :] = layer_norm(values, gain_ref[...], bias_ref[...]).astype(BF16)
 
@@ -579,7 +584,7 @@
         out_shape=shape_of((rows_here, chunks * LANES), BF16),
         in_specs=[VMEM, VMEM, SMEM, SMEM, VMEM, VMEM],
         out_specs=VMEM,
-        scratch_shapes=[pltpu.VMEM((rows_here * chunks, LANES), F32)],
+        scratch_shapes=[pltpu.VMEM((rows_here * PITCH, LANES), F32)],
         compiler_params=limit(8),
         name="final_rows",
     )(held(returned), middle, slots, weights, gain, bias)

time: 273 us -> 271 us (level)
  no operation moved by 1% of the time
where the time goes in v3:
time: 271 us; the launch traced here: 270 us
  waiting for transfers between devices  123 us (45%)
  blocking collectives  72.1 us (27%)
  Pallas kernels  33 us (12%)
  starting transfers between devices  31.3 us (12%)
  local copies, waits for them, and re-layouts  10.9 us (4%)
    ppermute x8, waiting for transfers between devices, turned_by(): lax.ppermute(value, 'tp', [(i, (i + distance) % peers) for i in range(pee...  114 us
    all_to_all x2, blocking collectives, exchanged(): return lax.all_to_all(value, axis, split_axis=0, concat_axis=0, tiled=True)  72.1 us
    all_to_all x3, starting transfers between devices, exchanged(): return lax.all_to_all(value, axis, split_axis=0, concat_axis=0, tiled=True)  15.9 us
    ppermute x8, starting transfers between devices, turned_by(): lax.ppermute(value, 'tp', [(i, (i + distance) % peers) for i in range(pee...  13.3 us
    unnamed x56, local copies, waits for them, and re-layouts  10.7 us
    pallas_call x1, Pallas kernels, expert_answers(): pl.pallas_call(lambda *refs: expert_kernel(places, *refs), out_shape=shap...  6.98 us
    all_to_all x3, waiting for transfers between devices, exchanged(): return lax.all_to_all(value, axis, split_axis=0, concat_axis=0, tiled=True)  5.69 us
    pallas_call x2, Pallas kernels, moved(): pl.pallas_call(lambda *refs: moved_kernel(moves, *refs), out_shape=tuple(...  5.63 us
  transfers between devices with their start and end apart: 12, of which 5 were waited for; matrix products, arithmetic and copies ran while one was open for 0% of the time, Pallas kernels for 4%

profile of v3, /device:TPU:8, one launch (start us, length us, event | category | flops | bytes accessed | tf_op | source)
XLA Modules:
  0.0 270.5 jit_solution(11569361140161236128)
XLA Ops:
  1.4 2.1 collective-permute-start.2
  3.4 3.2 %collective-permute-done.2.tail_ref = bf16[8,1536]{1,0:T(8,128)(2,1)S(1)} collective-permute-done((bf16[8,1536]{1,0:T(8,128)(2,1)S(1)}, bf16[8,1536]{1,0:T(8,128)(2,1)S(1)}, u32[]{:S(2)}, u32[]{:S(2)}) %collective-permute-start.2) | collective-permute-done | bytes 24608 | tf_op jit(solution)/shard_map/ppermute | solution.py:649
  6.7 4.3 %end_states.1 = (bf16[384,1024]{1,0:T(8,128)(2,1)}, bf16[384,1024]{1,0:T(8,128)(2,1)}, bf16[384,256]{1,0:T(8,128)(2,1)}, f32[384,16]{1,0:T(8,128)}, f32[2,2,128,...) custom-call(bf16[384,1024]{1,0:T(8,128)(2,1)S(1)} %get-tuple-element.35.x_ref, ...), custom_call_target="tpu_custom_call" | custom-call | tf_op jit(solution)/shard_map/end_states/pallas_call | solution.py:178
  10.9 27.4 %all_to_all.25.parts_ref = bf16[64,24,128]{2,1,0:T(8,128)(2,1)S(1)} all-to-all(bf16[64,24,128]{2,1,0:T(8,128)(2,1)S(1)} %get-tuple-element.51), channel_id=1, replica_groups=mesh['sp'=64,'tp'=4] {'sp'}, dimensions={0} | all-to-all | bytes 786432 | tf_op jit(solution)/shard_map/all_to_all | solution.py:599
  39.3 5.9 %all-to-all-start.1 = ((bf16[64,16,128]{2,1,0:T(8,128)(2,1)}), bf16[64,16,128]{2,1,0:T(8,128)(2,1)S(1)}, u32[]{:S(2)}, u32[]{:S(2)}) async-start(bf16[64,16,128]{2,1,0:T(8,128)(2,1)} %chain.1), calls=%async_computation.1 | async-start | bytes 524288 | tf_op jit(solution)/shard_map/all_to_all | solution.py:599
  48.9 2.2 local_outputs.1
  51.7 5.7 %all-to-all-done.1.incoming_ref = bf16[64,16,128]{2,1,0:T(8,128)(2,1)S(1)} async-done(((bf16[64,16,128]{2,1,0:T(8,128)(2,1)}), bf16[64,16,128]{2,1,0:T(8,128)(2,1)S(1)}, u32[]{:S(2)}, u32[]{:S(2)}) %all-to-all-start.1) | async-done | bytes 262176 | tf_op jit(solution)/shard_map/all_to_all | solution.py:599
  58.4 4.8 %projected.1 = bf16[384,2048]{1,0:T(8,128)(2,1)} custom-call(bf16[384,1024]{1,0:T(8,128)(2,1)S(1)} %get-tuple-element.48.fixed_ref, bf16[384,1024]{1,0:T(8,128)(2,1)S(1)} %get-tuple-element.49.factor_ref, bf16[384,256]{1,0:T(8,128)(2,1)S(1)} %copy-done.9, bf16[64,16,128]{2,1,0:T(8,128)(2,1)S(1)} %all-to-all-done.1.incoming_ref, ...), custom_call_target="tpu_custom_call" | custom-call | tf_op jit(solution)/shard_map/projected/pallas_call | solution.py:334
  63.2 4.4 %all-to-all-start.2 = ((bf16[4,96,2048]{2,1,0:T(8,128)(2,1)}), bf16[4,96,2048]{2,1,0:T(8,128)(2,1)S(1)}, u32[]{:S(2)}, u32[]{:S(2)}) async-start(bf16[4,96,2048]{2,1,0:T(8,128)(2,1)} %bitcast.6), calls=%async_computation.2 | async-start | bytes 3145728 | tf_op jit(solution)/shard_map/all_to_all | solution.py:599
  67.7 2.0 collective-permute-start
  70.9 2.2 slot_layout.1.refs_4_.refs_2_
  73.2 37.7 %collective-permute-done.refs_0_.refs_4_ = bf16[2048,256]{1,0:T(8,128)(2,1)S(1)} collective-permute-done((bf16[2048,256]{1,0:T(8,128)(2,1)S(1)}, bf16[2048,256]{1,0:T(8,128)(2,1)S(1)}, u32[]{:S(2)}, u32[]{:S(2)}) %collective-permute-start) | collective-permute-done | bytes 1048608 | tf_op jit(solution)/shard_map/ppermute | solution.py:595
  112.9 3.6 %moved.2 = (bf16[4096,256]{1,0:T(8,128)(2,1)}, bf16[4096,256]{1,0:T(8,128)(2,1)}) custom-call(bf16[2048,256]{1,0:T(8,128)(2,1)} %copy-done.20, bf16[2048,256]{1,0:T(8,128)(2,1)} %bitcast.31, bf16[2048,256]{1,0:T(8,128)(2,1)} %copy-done.21, bf16[2048,256]{1,0:T(8,128)(2,1)} %bitcast.27), custom_call_target="tpu_custom_call" | custom-call | tf_op jit(solution)/shard_map/moved/pallas_call | solution.py:546
  116.5 2.5 middle_rows.1
  119.0 5.6 %all-to-all-start.3 = ((bf16[64,80,128]{2,1,0:T(8,128)(2,1)}), bf16[64,80,128]{2,1,0:T(8,128)(2,1)S(1)}, u32[]{:S(2)}, u32[]{:S(2)}) async-start(bf16[64,80,128]{2,1,0:T(8,128)(2,1)} %bitcast.10), calls=%async_computation.3 | async-start | bytes 2621440 | tf_op jit(solution)/shard_map/all_to_all | solution.py:599
  124.9 3.2 %collective-permute-start.8 = (bf16[4096,256]{1,0:T(8,128)(2,1)}, bf16[4096,256]{1,0:T(8,128)(2,1)}, u32[]{:S(2)}, u32[]{:S(2)}) collective-permute-start(bf16[4096,256]{1,0:T(8,128)(2,1)} %get-tuple-element.57), channel_id=1, source_target_pairs={{0,3},{1,0},{2,1},{3,2},{4,7},{5,4},{6,5},{7,6},{8,11},{9,8},{10,9... | collective-permute-start | bytes 6291464 | tf_op jit(solution)/shard_map/ppermute | solution.py:595
  128.1 3.2 %collective-permute-start.4 = (bf16[2048,256]{1,0:T(8,128)(2,1)S(1)}, bf16[2048,256]{1,0:T(8,128)(2,1)S(1)}, u32[]{:S(2)}, u32[]{:S(2)}) collective-permute-start(bf16[2048,256]{1,0:T(8,128)(2,1)S(1)} %bitcast.35), channel_id=1, source_target_pairs={{0,3},{1,0},{2,1},{3,2},{4,7},{5,4},{6,5},{7,6},{8,11},{9,8},{10,9... | collective-permute-start | bytes 3145736 | tf_op jit(solution)/shard_map/ppermute | solution.py:595
  131.4 65.1 %collective-permute-done.3.refs_0_.refs_5_ = bf16[2048,256]{1,0:T(8,128)(2,1)S(1)} collective-permute-done((bf16[2048,256]{1,0:T(8,128)(2,1)S(1)}, bf16[2048,256]{1,0:T(8,128)(2,1)S(1)}, u32[]{:S(2)}, u32[]{:S(2)}) %collective-permute-start.3) | collective-permute-done | bytes 1048608 | tf_op jit(solution)/shard_map/ppermute | solution.py:595
  198.4 2.0 moved.3
  200.5 3.2 %collective-permute-start.6 = (bf16[1024,256]{1,0:T(8,128)(2,1)}, bf16[1024,256]{1,0:T(8,128)(2,1)S(1)}, u32[]{:S(2)}, u32[]{:S(2)}) collective-permute-start(bf16[1024,256]{1,0:T(8,128)(2,1)} %get-tuple-element.55), channel_id=1, source_target_pairs={{0,3},{1,0},{2,1},{3,2},{4,7},{5,4},{6,5},{7,6},{8,11},{9,8},{10,9... | collective-permute-start | bytes 1572872 | tf_op jit(solution)/shard_map/ppermute | solution.py:595
  203.8 11.3 %collective-permute-done.5.refs_8_ = bf16[1024,256]{1,0:T(8,128)(2,1)S(1)} collective-permute-done((bf16[1024,256]{1,0:T(8,128)(2,1)}, bf16[1024,256]{1,0:T(8,128)(2,1)S(1)}, u32[]{:S(2)}, u32[]{:S(2)}) %collective-permute-start.5) | collective-permute-done | bytes 524320 | tf_op jit(solution)/shard_map/ppermute | solution.py:595
  216.7 7.0 %expert_answers.1 = bf16[320,16,128]{2,1,0:T(8,128)(2,1)S(1)} custom-call(bf16[320,16,128]{2,1,0:T(8,128)(2,1)S(1)} %bitcast.19, bf16[2048,256]{1,0:T(8,128)(2,1)} %bitcast.28, bf16[2048,256]{1,0:T(8,128)(2,1)} %bitcast.33, bf16[2048,256]{1,0:T(8,128)(2,1)} %bitcast.32, bf16[2048,256]{1,0:T(8,128)(2,1)} %copy-done.20, bf16[2048,256]{1,0:T(8,128)(2,1)} %copy-done.17, ...), custom_call_target="tpu_custom_call" | custom-call | tf_op jit(solution)/shard_map/expert_answers/pallas_call | solution.py:469
  223.7 44.6 %all_to_all.26 = bf16[64,80,128]{2,1,0:T(8,128)(2,1)S(1)} all-to-all(bf16[64,80,128]{2,1,0:T(8,128)(2,1)S(1)} %bitcast.20), channel_id=1, replica_groups=mesh['sp'=64,'tp'=4] {'sp'}, dimensions={0} | all-to-all | bytes 2621440 | tf_op jit(solution)/shard_map/all_to_all | solution.py:599
  268.4 2.1 final_rows.1
  (72 shorter events, 14.7 us)
Async XLA Ops:
  1.3 43.9 %copy-start.27 = (f32[16]{0:T(128)S(1)}, f32[16]{0:T(128)}, u32[]{:S(2)}) copy-start(f32[16]{0:T(128)} %param.35) | copy-start | bytes 196
  1.3 44.1 %copy-start.26 = (bf16[1024]{0:T(1024)(128)(2,1)S(1)}, bf16[1024]{0:T(1024)(128)(2,1)}, u32[]{:S(2)}) copy-start(bf16[1024]{0:T(1024)(128)(2,1)} %param.36) | copy-start | bytes 6148
  1.4 44.1 %copy-start.1 = (bf16[384,256]{1,0:T(8,128)(2,1)S(1)}, bf16[384,256]{1,0:T(8,128)(2,1)}, u32[]{:S(2)}) copy-start(bf16[384,256]{1,0:T(8,128)(2,1)} %c_ref.1) | copy-start | bytes 589828
  1.4 44.1 %copy-start.14 = (bf16[4,256]{1,0:T(4,128)(2,1)S(1)}, bf16[4,256]{1,0:T(4,128)(2,1)}, u32[]{:S(2)}) copy-start(bf16[4,256]{1,0:T(4,128)(2,1)} %cf_ref.1) | copy-start | bytes 6148
  1.4 5.3 %collective-permute-start.2 = (bf16[8,1536]{1,0:T(8,128)(2,1)S(1)}, bf16[8,1536]{1,0:T(8,128)(2,1)S(1)}, u32[]{:S(2)}, u32[]{:S(2)}) collective-permute-start(bf16[8,1536]{1,0:T(8,128)(2,1)S(1)} %get-tuple-element.34), channel_id=1, source_target_pairs={{0,4},{4,8},{8,12},{12,16},{16,20},{20,24},{24,28},{28,32},{32,36}... | collective-permute-start | bytes 73736 | tf_op jit(solution)/shard_map/ppermute | solution.py:649
  10.9 34.5 %copy-start.6 = (bf16[384,256]{1,0:T(8,128)(2,1)S(1)}, bf16[384,256]{1,0:T(8,128)(2,1)}, u32[]{:S(2)}) copy-start(bf16[384,256]{1,0:T(8,128)(2,1)} %get-tuple-element.43.bc_ref) | copy-start | bytes 589828
  10.9 34.5 %copy-start.7 = (f32[384,16]{1,0:T(8,128)S(1)}, f32[384,16]{1,0:T(8,128)}, u32[]{:S(2)}) copy-start(f32[384,16]{1,0:T(8,128)} %get-tuple-element.46.running_ref) | copy-start | bytes 73732
  39.3 18.1 %all-to-all-start.1 = ((bf16[64,16,128]{2,1,0:T(8,128)(2,1)}), bf16[64,16,128]{2,1,0:T(8,128)(2,1)S(1)}, u32[]{:S(2)}, u32[]{:S(2)}) async-start(bf16[64,16,128]{2,1,0:T(8,128)(2,1)} %chain.1), calls=%async_computation.1 | async-start | bytes 524288 | tf_op jit(solution)/shard_map/all_to_all | solution.py:599
  63.2 53.3 %all-to-all-start.2 = ((bf16[4,96,2048]{2,1,0:T(8,128)(2,1)}), bf16[4,96,2048]{2,1,0:T(8,128)(2,1)S(1)}, u32[]{:S(2)}, u32[]{:S(2)}) async-start(bf16[4,96,2048]{2,1,0:T(8,128)(2,1)} %bitcast.6), calls=%async_computation.2 | async-start | bytes 3145728 | tf_op jit(solution)/shard_map/all_to_all | solution.py:599
  67.7 43.2 %collective-permute-start = (bf16[2048,256]{1,0:T(8,128)(2,1)S(1)}, bf16[2048,256]{1,0:T(8,128)(2,1)S(1)}, u32[]{:S(2)}, u32[]{:S(2)}) collective-permute-start(bf16[2048,256]{1,0:T(8,128)(2,1)S(1)} %bitcast.29), channel_id=1, source_target_pairs={{0,1},{1,2},{2,3},{3,0},{4,5},{5,6},{6,7},{7,4},{8,9},{9,10},{10,1... | collective-permute-start | bytes 3145736 | tf_op jit(solution)/shard_map/ppermute | solution.py:595
  69.7 41.2 %collective-permute-start.1 = (bf16[2048,256]{1,0:T(8,128)(2,1)}, bf16[2048,256]{1,0:T(8,128)(2,1)S(1)}, u32[]{:S(2)}, u32[]{:S(2)}) collective-permute-start(bf16[2048,256]{1,0:T(8,128)(2,1)} %bitcast.30), channel_id=1, source_target_pairs={{0,3},{1,0},{2,1},{3,2},{4,7},{5,4},{6,5},{7,6},{8,11},{9,8},{10,9... | collective-permute-start | bytes 3145736 | tf_op jit(solution)/shard_map/ppermute | solution.py:595
  73.1 43.4 %copy-start.5 = (bf16[96,2048]{1,0:T(8,128)(2,1)S(1)}, bf16[96,2048]{1,0:T(8,128)(2,1)}, u32[]{:S(2)}) copy-start(bf16[96,2048]{1,0:T(8,128)(2,1)} %refs_1_.3) | copy-start | bytes 1179652
  73.2 43.4 %copy-start.10 = (f32[2048]{0:T(1024)S(1)}, f32[2048]{0:T(1024)}, u32[]{:S(2)}) copy-start(f32[2048]{0:T(1024)} %param.39) | copy-start | bytes 24580
  73.2 43.4 %copy-start.11 = (f32[2048]{0:T(1024)S(1)}, f32[2048]{0:T(1024)}, u32[]{:S(2)}) copy-start(f32[2048]{0:T(1024)} %param.40) | copy-start | bytes 24580
  119.0 97.4 %all-to-all-start.3 = ((bf16[64,80,128]{2,1,0:T(8,128)(2,1)}), bf16[64,80,128]{2,1,0:T(8,128)(2,1)S(1)}, u32[]{:S(2)}, u32[]{:S(2)}) async-start(bf16[64,80,128]{2,1,0:T(8,128)(2,1)} %bitcast.10), calls=%async_computation.3 | async-start | bytes 2621440 | tf_op jit(solution)/shard_map/all_to_all | solution.py:599
  124.6 90.4 %collective-permute-start.7 = (bf16[4096,256]{1,0:T(8,128)(2,1)}, bf16[4096,256]{1,0:T(8,128)(2,1)S(1)}, u32[]{:S(2)}, u32[]{:S(2)}) collective-permute-start(bf16[4096,256]{1,0:T(8,128)(2,1)} %get-tuple-element.56), channel_id=1, source_target_pairs={{0,1},{1,2},{2,3},{3,0},{4,5},{5,6},{6,7},{7,4},{8,9},{9,10},{10,1... | collective-permute-start | bytes 6291464 | tf_op jit(solution)/shard_map/ppermute | solution.py:595
  124.9 91.5 %collective-permute-start.8 = (bf16[4096,256]{1,0:T(8,128)(2,1)}, bf16[4096,256]{1,0:T(8,128)(2,1)}, u32[]{:S(2)}, u32[]{:S(2)}) collective-permute-start(bf16[4096,256]{1,0:T(8,128)(2,1)} %get-tuple-element.57), channel_id=1, source_target_pairs={{0,3},{1,0},{2,1},{3,2},{4,7},{5,4},{6,5},{7,6},{8,11},{9,8},{10,9... | collective-permute-start | bytes 6291464 | tf_op jit(solution)/shard_map/ppermute | solution.py:595
  128.1 68.3 %collective-permute-start.3 = (bf16[2048,256]{1,0:T(8,128)(2,1)S(1)}, bf16[2048,256]{1,0:T(8,128)(2,1)S(1)}, u32[]{:S(2)}, u32[]{:S(2)}) collective-permute-start(bf16[2048,256]{1,0:T(8,128)(2,1)S(1)} %bitcast.34), channel_id=1, source_target_pairs={{0,1},{1,2},{2,3},{3,0},{4,5},{5,6},{6,7},{7,4},{8,9},{9,10},{10,1... | collective-permute-start | bytes 3145736 | tf_op jit(solution)/shard_map/ppermute | solution.py:595
  128.1 68.3 %collective-permute-start.4 = (bf16[2048,256]{1,0:T(8,128)(2,1)S(1)}, bf16[2048,256]{1,0:T(8,128)(2,1)S(1)}, u32[]{:S(2)}, u32[]{:S(2)}) collective-permute-start(bf16[2048,256]{1,0:T(8,128)(2,1)S(1)} %bitcast.35), channel_id=1, source_target_pairs={{0,3},{1,0},{2,1},{3,2},{4,7},{5,4},{6,5},{7,6},{8,11},{9,8},{10,9... | collective-permute-start | bytes 3145736 | tf_op jit(solution)/shard_map/ppermute | solution.py:595
  200.5 14.6 %collective-permute-start.5 = (bf16[1024,256]{1,0:T(8,128)(2,1)}, bf16[1024,256]{1,0:T(8,128)(2,1)S(1)}, u32[]{:S(2)}, u32[]{:S(2)}) collective-permute-start(bf16[1024,256]{1,0:T(8,128)(2,1)} %get-tuple-element.54), channel_id=1, source_target_pairs={{0,1},{1,2},{2,3},{3,0},{4,5},{5,6},{6,7},{7,4},{8,9},{9,10},{10,1... | collective-permute-start | bytes 1572872 | tf_op jit(solution)/shard_map/ppermute | solution.py:595
  200.5 14.5 %collective-permute-start.6 = (bf16[1024,256]{1,0:T(8,128)(2,1)}, bf16[1024,256]{1,0:T(8,128)(2,1)S(1)}, u32[]{:S(2)}, u32[]{:S(2)}) collective-permute-start(bf16[1024,256]{1,0:T(8,128)(2,1)} %get-tuple-element.55), channel_id=1, source_target_pairs={{0,3},{1,0},{2,1},{3,2},{4,7},{5,4},{6,5},{7,6},{8,11},{9,8},{10,9... | collective-permute-start | bytes 1572872 | tf_op jit(solution)/shard_map/ppermute | solution.py:595
  223.7 44.7 %copy-start.12 = (f32[2048]{0:T(1024)S(1)}, f32[2048]{0:T(1024)}, u32[]{:S(2)}) copy-start(f32[2048]{0:T(1024)} %param.46) | copy-start | bytes 24580
  223.7 44.7 %copy-start.13 = (f32[2048]{0:T(1024)S(1)}, f32[2048]{0:T(1024)}, u32[]{:S(2)}) copy-start(f32[2048]{0:T(1024)} %param.47) | copy-start | bytes 24580
  223.7 44.6 %copy-start.15 = (f32[96,2]{0,1:T(2,128)S(1)}, f32[96,2]{0,1:T(2,128)}, u32[]{:S(2)}) copy-start(f32[96,2]{0,1:T(2,128)} %param.42) | copy-start | bytes 2308
  (16 other events, 69.4 us)

commit v4 on v3

--- a/solution.py
+++ b/solution.py
@@ -1,3 +1,5 @@
+import math
+
 import jax
 import jax.numpy as jnp
 from jax import lax
@@ -106,12 +108,11 @@
     extra_ref,
     bias_ref,
     rate_ref,
-    xc_ref,
-    xdt_ref,
     bc_ref,
     running_ref,
     states_ref,
     message_ref,
+    xc_ref,
     rows_ref,
 ):
     length, channels = x_ref.shape
@@ -123,8 +124,10 @@
     step, decay = log_decays(logits_ref, extra_ref, bias_ref, rate_ref)
     sums = []
     for i in range(blocks):
-        part = running_sum(decay[i * BLOCK : (i + 1) * BLOCK])
-        running_ref[i * BLOCK : (i + 1) * BLOCK, :] = part
+        rows = slice(i * BLOCK, (i + 1) * BLOCK)
+        part = running_sum(decay[rows])
+        running_ref[0, rows, :] = part
+        running_ref[1, rows, :] = step[rows]
         sums.append(part)
     for c in range(0, groups * STATE_WIDTH, LANES):
         cols = slice(c, c + LANES)
@@ -147,7 +150,6 @@
             step_wide = spread_heads(step[rows], g, heads, width)
             left_wide = spread_heads(jnp.exp(ending - sums[i]), g, heads, width)
             scaled = xc_ref[rows, here].astype(F32) * step_wide
-            xdt_ref[rows, here] = scaled.astype(BF16)
             keys = bc_ref[rows, g * STATE_WIDTH : (g + 1) * STATE_WIDTH].astype(F32).T.astype(BF16)
             added = dot(keys, (scaled * left_wide).astype(BF16))
             if state is None:
@@ -155,7 +157,7 @@
             else:
                 state = state * spread_heads(jnp.exp(ending), g, heads, width) + added
             if i + 1 < blocks:
-                states_ref[i, g] = state
+                states_ref[i, g] = state.astype(BF16)
         high = total.astype(BF16)
         rest = total - high.astype(F32)
         low = rest.astype(BF16)
@@ -178,16 +180,14 @@
     return pl.pallas_call(
         end_state_kernel,
         out_shape=(
-            pltpu.HBM((length, channels), BF16),
-            pltpu.HBM((length, channels), BF16),
             pltpu.HBM(b.shape, BF16),
-            pltpu.HBM((length, logits.shape[0]), F32),
-            pltpu.HBM((blocks - 1, groups, STATE_WIDTH, width), F32),
-            shape_of((pieces, 24, LANES), BF16),
+            pltpu.HBM((2, length, logits.shape[0]), F32),
+            pltpu.HBM((blocks - 1, groups, STATE_WIDTH, width), BF16),
+            near((pieces, 24, LANES), BF16),
         ),
         in_specs=[VMEM] * 9,
-        out_specs=(VMEM,) * 6,
-        scratch_shapes=[pltpu.VMEM((8 + length, LANES), F32)],
+        out_specs=(VMEM,) * 4,
+        scratch_shapes=[pltpu.VMEM((length, channels), BF16), pltpu.VMEM((8 + length, LANES), F32)],
         compiler_params=limit(12),
         name="end_states",
     )(*map(held, (x, b, tail, xf, bf, logits, extra, bias, rate)))
@@ -221,8 +221,8 @@
     tail_ref,
     cf_ref,
     bc_ref,
-    xdt_ref,
-    xc_ref,
+    x_ref,
+    xf_ref,
     running_ref,
     states_ref,
     direct_ref,
@@ -230,9 +230,10 @@
     cc_ref,
     fixed_ref,
     factor_ref,
+    xc_ref,
     rows_ref,
 ):
-    length, channels = xdt_ref.shape
+    length, channels = x_ref.shape
     margin = cf_ref.shape[0] - 1
     groups = bc_ref.shape[1] // STATE_WIDTH
     width = channels // groups
@@ -242,14 +243,18 @@
         cols = slice(c, c + LANES)
         fill_rows(rows_ref, tail_ref, c_ref, cols, offset, length)
         cc_ref[:, cols] = conv_cols(rows_ref, cf_ref[:, cols].astype(F32), length, margin).astype(BF16)
+    for c in range(0, channels, LANES):
+        cols = slice(c, c + LANES)
+        fill_rows(rows_ref, tail_ref, x_ref, cols, 0, length)
+        xc_ref[:, cols] = conv_cols(rows_ref, xf_ref[:, cols].astype(F32), length, margin).astype(BF16)
     t = lax.broadcasted_iota(jnp.int32, (BLOCK, BLOCK), 0)
     s = lax.broadcasted_iota(jnp.int32, (BLOCK, BLOCK), 1)
     causal = t >= s
     first_head = lax.broadcasted_iota(jnp.int32, (BLOCK, LANES), 1) < HEAD_DIM
-    started = jnp.zeros((1, running_ref.shape[1]), F32)
+    started = jnp.zeros((1, running_ref.shape[2]), F32)
     for i in range(length // BLOCK):
         rows = slice(i * BLOCK, (i + 1) * BLOCK)
-        running = running_ref[rows, :]
+        running, step = running_ref[0, rows, :], running_ref[1, rows, :]
         padded = jnp.concatenate([running, jnp.zeros((BLOCK, BLOCK - running.shape[1]), F32)], axis=1)
         across = padded.T
         since_block = jnp.exp(running)
@@ -262,15 +267,17 @@
             products = jnp.where(causal, products, 0.0)
             gate = silu(gate_ref[rows, here].astype(F32))
             factor_ref[rows, here] = (spread_heads(since_start, g, heads, width) * gate).astype(BF16)
+            inputs = xc_ref[rows, here].astype(F32)
+            scaled = (inputs * spread_heads(step, g, heads, width)).astype(BF16)
             carried = None
             if i > 0:
-                read = dot(cc_ref[rows, wide], states_ref[i - 1, g].astype(BF16))
+                read = dot(cc_ref[rows, wide], states_ref[i - 1, g])
                 carried = read * spread_heads(since_block, g, heads, width)
             for p in range(width // LANES):
                 part = slice(p * LANES, (p + 1) * LANES)
                 cols = slice(g * width + p * LANES, g * width + (p + 1) * LANES)
-                pair = xdt_ref[rows, cols]
-                total = direct_ref[:, cols] * xc_ref[rows, cols].astype(F32)
+                pair = scaled[:, part]
+                total = direct_ref[:, cols] * inputs[:, part]
                 if carried is not None:
                     total = total + carried[:, part]
                 for q in range(LANES // HEAD_DIM):
@@ -282,8 +289,8 @@
                 fixed_ref[rows, cols] = (total * gate[:, part]).astype(BF16)
 
 
-def local_outputs(c, tail, cf, bc, xdt, xc, running, states, direct, gate):
-    length, channels = xdt.shape
+def local_outputs(c, tail, cf, bc, x, xf, running, states, direct, gate):
+    length, channels = x.shape
     return pl.pallas_call(
         local_kernel,
         out_shape=(
@@ -293,10 +300,10 @@
         ),
         in_specs=[VMEM] * 10,
         out_specs=(VMEM,) * 3,
-        scratch_shapes=[pltpu.VMEM((8 + length, LANES), F32)],
+        scratch_shapes=[pltpu.VMEM((length, channels), BF16), pltpu.VMEM((8 + length, LANES), F32)],
         compiler_params=limit(14),
         name="local_outputs",
-    )(c, tail, cf, bc, xdt, xc, running, states, direct, gate)
+    )(c, tail, cf, bc, x, xf, running, states, direct, gate)
 
 
 def project_kernel(fixed_ref, factor_ref, cc_ref, incoming_ref, scale_ref, w_hbm, out_ref, w_ref, rows_ref, read_ref, sem):
@@ -431,9 +438,11 @@
     width = chunks * LANES
     quarters, _, units = buffer_ref.shape
     copies = []
-    for n, (which, at, size, quarter, to) in enumerate(places):
+    ordered = sorted(places, key=lambda place: place[4] >= 2 * width)
+    for n, (which, at, size, quarter, to) in enumerate(ordered):
         source = pieces[which].at[pl.ds(at, size)]
-        copies.append((quarter, pltpu.make_async_copy(source, buffer_ref.at[quarter, pl.ds(to, size)], sem.at[n])))
+        copy = pltpu.make_async_copy(source, buffer_ref.at[quarter, pl.ds(to, size)], sem.at[n])
+        copies.append((quarter if to < 2 * width else quarters, copy))
     for _, copy in copies:
         copy.start()
     for s in range(0, slots, 16):
@@ -448,6 +457,9 @@
         gate = dot(x_ref[...], buffer_ref[q, :width, :])
         up = dot(x_ref[...], buffer_ref[q, width : 2 * width, :])
         hidden_ref[:, q * units : (q + 1) * units] = (silu(gate) * up).astype(BF16)
+    for quarter, copy in copies:
+        if quarter == quarters:
+            copy.wait()
     step = 512
     for n in range(0, width, step):
         total = None
@@ -540,7 +552,7 @@
 
 def moved(values, *moves):
     units = values[0].shape[1]
-    step = min(size for parts in moves for _, _, size in parts) // 2
+    step = math.gcd(*(size for parts in moves for _, _, size in parts))
     rows = [sum(size for _, _, size in parts) for parts in moves]
     count = sum(rows) // step
     return pl.pallas_call(
@@ -652,7 +664,7 @@
     up_ahead = turned_by(up, -1)
     gate_behind = turned_by(gate, 1)
     down_ahead = turned_by(down, -1)
-    xc, xdt, bc, running, states, message = end_states(tail, *entering)
+    bc, running, states, message = end_states(tail, *entering)
     met = exchanged(message, SP)
     slots = slot_layout(routes.T, capacity, experts)
     direct = jnp.repeat(direct_path_weight, HEAD_DIM)[None]
@@ -661,8 +673,8 @@
         tail,
         readout_vector_filter,
         bc,
-        xdt,
-        xc,
+        head_input_values,
+        head_input_filter,
         running,
         states,
         direct,
@@ -670,7 +682,12 @@
     )
     incoming = exchanged(chain(met), SP)
     half = width // 2
-    low, high = moved((up_behind, up_ahead), ((0, 0, half),), ((1, half, half),))
+    extra = width // 8
+    low, high = moved(
+        (up_behind, down, up_ahead, gate),
+        ((0, 0, half), (1, 0, extra)),
+        ((2, half, half), (3, 0, extra)),
+    )
     up_low = turned_by(low, 1)
     up_high = turned_by(high, -1)
     sums = projected(fixed, factor, cc, incoming, group_norm_scale[None], mixer_output_weight)
@@ -678,8 +695,8 @@
     parts = exchanged(sums.reshape(peers, rows_here, width), "tp")
     onward = moved(
         (gate_behind, down, down_ahead, gate),
-        ((0, 0, width), (1, 0, width)),
-        ((2, 0, width), (3, 0, width)),
+        ((0, 0, width), (1, extra, width - extra)),
+        ((2, 0, width), (3, extra, width - extra)),
     )
     onward, parts = lax.optimization_barrier((onward, parts))
     last_on = turned_by(onward[0], 1)
@@ -698,8 +715,10 @@
             (2, 0, width, 0, 2 * width),
             (3, 0, width, 1, 0),
             (4, 0, width, 1, width),
-            (9, width, width, 1, 2 * width),
-            (10, width, width, 2, 0),
+            (7, half, extra, 1, 2 * width),
+            (9, width, width - extra, 1, 2 * width + extra),
+            (8, half, extra, 2, 0),
+            (10, width, width - extra, 2, extra),
             (5, 0, width, 2, width),
             (6, 0, width, 2, 2 * width),
             (9, 0, width, 3, 0),

time: 271 us -> 272 us (level)
  transfers between devices with their start and end apart: 12 -> 12, of which waited for: 5 -> 5; matrix products, arithmetic and copies ran while one was open for 0% -> 0% of each run, Pallas kernels for 4% -> 5%
where the time goes in v4:
time: 272 us; the launch traced here: 271 us
  waiting for transfers between devices  121 us (44%)
  blocking collectives  71.9 us (26%)
  Pallas kernels  34.1 us (13%)
  starting transfers between devices  32.1 us (12%)
  local copies, waits for them, and re-layouts  11.5 us (4%)
    ppermute x8, waiting for transfers between devices, turned_by(): lax.ppermute(value, 'tp', [(i, (i + distance) % peers) for i in range(pee...  114 us
    all_to_all x2, blocking collectives, exchanged(): return lax.all_to_all(value, axis, split_axis=0, concat_axis=0, tiled=True)  71.9 us
    all_to_all x3, starting transfers between devices, exchanged(): return lax.all_to_all(value, axis, split_axis=0, concat_axis=0, tiled=True)  16.9 us
    ppermute x8, starting transfers between devices, turned_by(): lax.ppermute(value, 'tp', [(i, (i + distance) % peers) for i in range(pee...  13.1 us
    unnamed x56, local copies, waits for them, and re-layouts  11.3 us
    pallas_call x1, Pallas kernels, expert_answers(): pl.pallas_call(lambda *refs: expert_kernel(places, *refs), out_shape=shap...  6.72 us
    pallas_call x2, Pallas kernels, moved(): pl.pallas_call(lambda *refs: moved_kernel(moves, *refs), out_shape=tuple(...  6.48 us
  transfers between devices with their start and end apart: 12, of which 5 were waited for; matrix products, arithmetic and copies ran while one was open for 0% of the time, Pallas kernels for 5%

profile of v4, /device:TPU:8, one launch (start us, length us, event | category | flops | bytes accessed | tf_op | source)
XLA Modules:
  0.0 271.0 jit_solution(8837008712022775661)
XLA Ops:
  1.4 2.1 collective-permute-start.2
  3.5 3.2 %collective-permute-done.2.tail_ref = bf16[8,1536]{1,0:T(8,128)(2,1)S(1)} collective-permute-done((bf16[8,1536]{1,0:T(8,128)(2,1)S(1)}, bf16[8,1536]{1,0:T(8,128)(2,1)S(1)}, u32[]{:S(2)}, u32[]{:S(2)}) %collective-permute-start.2) | collective-permute-done | bytes 24608 | tf_op jit(solution)/shard_map/ppermute | solution.py:661
  6.7 3.5 %end_states.1 = (bf16[384,256]{1,0:T(8,128)(2,1)}, f32[2,384,16]{2,1,0:T(8,128)}, bf16[2,2,128,512]{3,2,1,0:T(8,128)(2,1)}, bf16[64,24,128]{2,1,0:T(8,128)(2,1)S(1)}) custom-call(bf16[384,1024]{1,0:T(8,128)(2,1)S(1)} %get-tuple-element.33.x_ref, bf16[384,256]{1,0:T(8,128)(2,1)S(1)} %get-tuple-element.34.b_ref, ...), custom_call_target="tpu_custom_call" | custom-call | tf_op jit(solution)/shard_map/end_states/pallas_call | solution.py:180
  10.1 27.3 %all_to_all.25.parts_ref = bf16[64,24,128]{2,1,0:T(8,128)(2,1)S(1)} all-to-all(bf16[64,24,128]{2,1,0:T(8,128)(2,1)S(1)} %get-tuple-element.47), channel_id=1, replica_groups=mesh['sp'=64,'tp'=4] {'sp'}, dimensions={0} | all-to-all | bytes 786432 | tf_op jit(solution)/shard_map/all_to_all | solution.py:611
  38.4 5.9 %all-to-all-start.1 = ((bf16[64,16,128]{2,1,0:T(8,128)(2,1)}), bf16[64,16,128]{2,1,0:T(8,128)(2,1)S(1)}, u32[]{:S(2)}, u32[]{:S(2)}) async-start(bf16[64,16,128]{2,1,0:T(8,128)(2,1)} %chain.1), calls=%async_computation.1 | async-start | bytes 524288 | tf_op jit(solution)/shard_map/all_to_all | solution.py:611
  48.4 3.5 %local_outputs.1 = (bf16[384,256]{1,0:T(8,128)(2,1)S(1)}, bf16[384,1024]{1,0:T(8,128)(2,1)S(1)}, bf16[384,1024]{1,0:T(8,128)(2,1)S(1)}) custom-call(bf16[384,256]{1,0:T(8,128)(2,1)S(1)} %copy-done.2, bf16[8,1536]{1,0:T(8,128)(2,1)S(1)} %collective-permute-done.2.tail_ref, bf16[4,256]{1,0:T(4,128)(2,1)S(1)} %copy-done.14, bf16[384,256]{1,0:T(8,128)(2,1)S(1)} %copy-done.6, ...), custom_call_target="tpu_custom_call" | custom-call | tf_op jit(solution)/shard_map/local_outputs/pallas_call | solution.py:294
  52.6 3.9 %all-to-all-done.1.incoming_ref = bf16[64,16,128]{2,1,0:T(8,128)(2,1)S(1)} async-done(((bf16[64,16,128]{2,1,0:T(8,128)(2,1)}), bf16[64,16,128]{2,1,0:T(8,128)(2,1)S(1)}, u32[]{:S(2)}, u32[]{:S(2)}) %all-to-all-start.1) | async-done | bytes 262176 | tf_op jit(solution)/shard_map/all_to_all | solution.py:611
  57.4 4.8 %projected.1 = bf16[384,2048]{1,0:T(8,128)(2,1)} custom-call(bf16[384,1024]{1,0:T(8,128)(2,1)S(1)} %get-tuple-element.44.fixed_ref, bf16[384,1024]{1,0:T(8,128)(2,1)S(1)} %get-tuple-element.45.factor_ref, bf16[384,256]{1,0:T(8,128)(2,1)S(1)} %copy-done.8, bf16[64,16,128]{2,1,0:T(8,128)(2,1)S(1)} %all-to-all-done.1.incoming_ref, ...), custom_call_target="tpu_custom_call" | custom-call | tf_op jit(solution)/shard_map/projected/pallas_call | solution.py:341
  62.3 4.5 %all-to-all-start.2 = ((bf16[4,96,2048]{2,1,0:T(8,128)(2,1)}), bf16[4,96,2048]{2,1,0:T(8,128)(2,1)S(1)}, u32[]{:S(2)}, u32[]{:S(2)}) async-start(bf16[4,96,2048]{2,1,0:T(8,128)(2,1)} %bitcast.6), calls=%async_computation.2 | async-start | bytes 3145728 | tf_op jit(solution)/shard_map/all_to_all | solution.py:611
  66.8 2.0 collective-permute-start
  70.0 2.2 slot_layout.1.refs_4_.refs_2_
  72.3 37.7 %collective-permute-done.refs_0_.refs_4_ = bf16[2048,256]{1,0:T(8,128)(2,1)S(1)} collective-permute-done((bf16[2048,256]{1,0:T(8,128)(2,1)S(1)}, bf16[2048,256]{1,0:T(8,128)(2,1)S(1)}, u32[]{:S(2)}, u32[]{:S(2)}) %collective-permute-start) | collective-permute-done | bytes 1048608 | tf_op jit(solution)/shard_map/ppermute | solution.py:607
  112.0 4.2 %moved.2 = (bf16[3840,256]{1,0:T(8,128)(2,1)}, bf16[3840,256]{1,0:T(8,128)(2,1)}) custom-call(bf16[2048,256]{1,0:T(8,128)(2,1)} %copy-done.18, bf16[2048,256]{1,0:T(8,128)(2,1)} %bitcast.32, bf16[2048,256]{1,0:T(8,128)(2,1)} %copy-done.19, bf16[2048,256]{1,0:T(8,128)(2,1)} %bitcast.27), custom_call_target="tpu_custom_call" | custom-call | tf_op jit(solution)/shard_map/moved/pallas_call | solution.py:558
  116.3 2.5 middle_rows.1
  118.8 6.5 %all-to-all-start.3 = ((bf16[64,80,128]{2,1,0:T(8,128)(2,1)}), bf16[64,80,128]{2,1,0:T(8,128)(2,1)S(1)}, u32[]{:S(2)}, u32[]{:S(2)}) async-start(bf16[64,80,128]{2,1,0:T(8,128)(2,1)} %bitcast.10), calls=%async_computation.3 | async-start | bytes 2621440 | tf_op jit(solution)/shard_map/all_to_all | solution.py:611
  125.4 3.2 %collective-permute-start.8 = (bf16[3840,256]{1,0:T(8,128)(2,1)}, bf16[3840,256]{1,0:T(8,128)(2,1)}, u32[]{:S(2)}, u32[]{:S(2)}) collective-permute-start(bf16[3840,256]{1,0:T(8,128)(2,1)} %get-tuple-element.53), channel_id=1, source_target_pairs={{0,3},{1,0},{2,1},{3,2},{4,7},{5,4},{6,5},{7,6},{8,11},{9,8},{10,9... | collective-permute-start | bytes 5898248 | tf_op jit(solution)/shard_map/ppermute | solution.py:607
  128.6 3.2 %collective-permute-start.4 = (bf16[2048,256]{1,0:T(8,128)(2,1)S(1)}, bf16[2048,256]{1,0:T(8,128)(2,1)S(1)}, u32[]{:S(2)}, u32[]{:S(2)}) collective-permute-start(bf16[2048,256]{1,0:T(8,128)(2,1)S(1)} %bitcast.37), channel_id=1, source_target_pairs={{0,3},{1,0},{2,1},{3,2},{4,7},{5,4},{6,5},{7,6},{8,11},{9,8},{10,9... | collective-permute-start | bytes 3145736 | tf_op jit(solution)/shard_map/ppermute | solution.py:607
  131.9 62.3 %collective-permute-done.3.refs_0_.refs_5_ = bf16[2048,256]{1,0:T(8,128)(2,1)S(1)} collective-permute-done((bf16[2048,256]{1,0:T(8,128)(2,1)S(1)}, bf16[2048,256]{1,0:T(8,128)(2,1)S(1)}, u32[]{:S(2)}, u32[]{:S(2)}) %collective-permute-start.3) | collective-permute-done | bytes 1048608 | tf_op jit(solution)/shard_map/ppermute | solution.py:607
  196.1 2.3 moved.3
  198.5 3.2 %collective-permute-start.6 = (bf16[1280,256]{1,0:T(8,128)(2,1)}, bf16[1280,256]{1,0:T(8,128)(2,1)S(1)}, u32[]{:S(2)}, u32[]{:S(2)}) collective-permute-start(bf16[1280,256]{1,0:T(8,128)(2,1)} %get-tuple-element.51), channel_id=1, source_target_pairs={{0,3},{1,0},{2,1},{3,2},{4,7},{5,4},{6,5},{7,6},{8,11},{9,8},{10,9... | collective-permute-start | bytes 1966088 | tf_op jit(solution)/shard_map/ppermute | solution.py:607
  201.7 14.1 %collective-permute-done.5.refs_8_ = bf16[1280,256]{1,0:T(8,128)(2,1)S(1)} collective-permute-done((bf16[1280,256]{1,0:T(8,128)(2,1)}, bf16[1280,256]{1,0:T(8,128)(2,1)S(1)}, u32[]{:S(2)}, u32[]{:S(2)}) %collective-permute-start.5) | collective-permute-done | bytes 655392 | tf_op jit(solution)/shard_map/ppermute | solution.py:607
  217.5 6.7 %expert_answers.1 = bf16[320,16,128]{2,1,0:T(8,128)(2,1)S(1)} custom-call(bf16[320,16,128]{2,1,0:T(8,128)(2,1)S(1)} %bitcast.19, bf16[2048,256]{1,0:T(8,128)(2,1)} %bitcast.29, bf16[2048,256]{1,0:T(8,128)(2,1)} %bitcast.35, bf16[2048,256]{1,0:T(8,128)(2,1)} %bitcast.34, bf16[2048,256]{1,0:T(8,128)(2,1)} %copy-done.18, bf16[2048,256]{1,0:T(8,128)(2,1)} %copy-done.20, ...), custom_call_target="tpu_custom_call" | custom-call | tf_op jit(solution)/shard_map/expert_answers/pallas_call | solution.py:481
  224.3 44.6 %all_to_all.26 = bf16[64,80,128]{2,1,0:T(8,128)(2,1)S(1)} all-to-all(bf16[64,80,128]{2,1,0:T(8,128)(2,1)S(1)} %bitcast.20), channel_id=1, replica_groups=mesh['sp'=64,'tp'=4] {'sp'}, dimensions={0} | all-to-all | bytes 2621440 | tf_op jit(solution)/shard_map/all_to_all | solution.py:611
  268.9 2.1 final_rows.1
  (72 shorter events, 15.2 us)
Async XLA Ops:
  1.3 43.0 %copy-start.27 = (f32[16]{0:T(128)S(1)}, f32[16]{0:T(128)}, u32[]{:S(2)}) copy-start(f32[16]{0:T(128)} %param.35) | copy-start | bytes 196
  1.3 43.1 %copy-start.26 = (bf16[1024]{0:T(1024)(128)(2,1)S(1)}, bf16[1024]{0:T(1024)(128)(2,1)}, u32[]{:S(2)}) copy-start(bf16[1024]{0:T(1024)(128)(2,1)} %param.36) | copy-start | bytes 6148
  1.4 43.1 %copy-start = (bf16[384,1024]{1,0:T(8,128)(2,1)S(1)}, bf16[384,1024]{1,0:T(8,128)(2,1)}, u32[]{:S(2)}) copy-start(bf16[384,1024]{1,0:T(8,128)(2,1)} %x_ref.1) | copy-start | bytes 2359300
  1.4 43.1 %copy-start.1 = (bf16[384,1024]{1,0:T(8,128)(2,1)S(1)}, bf16[384,1024]{1,0:T(8,128)(2,1)}, u32[]{:S(2)}) copy-start(bf16[384,1024]{1,0:T(8,128)(2,1)} %gate_ref.1) | copy-start | bytes 2359300
  1.4 43.1 %copy-start.9 = (bf16[4,1024]{1,0:T(4,128)(2,1)S(1)}, bf16[4,1024]{1,0:T(4,128)(2,1)}, u32[]{:S(2)}) copy-start(bf16[4,1024]{1,0:T(4,128)(2,1)} %xf_ref.1) | copy-start | bytes 24580
  1.4 43.1 %copy-start.14 = (bf16[4,256]{1,0:T(4,128)(2,1)S(1)}, bf16[4,256]{1,0:T(4,128)(2,1)}, u32[]{:S(2)}) copy-start(bf16[4,256]{1,0:T(4,128)(2,1)} %cf_ref.1) | copy-start | bytes 6148
  1.4 5.3 %collective-permute-start.2 = (bf16[8,1536]{1,0:T(8,128)(2,1)S(1)}, bf16[8,1536]{1,0:T(8,128)(2,1)S(1)}, u32[]{:S(2)}, u32[]{:S(2)}) collective-permute-start(bf16[8,1536]{1,0:T(8,128)(2,1)S(1)} %get-tuple-element.32), channel_id=1, source_target_pairs={{0,4},{4,8},{8,12},{12,16},{16,20},{20,24},{24,28},{28,32},{32,36}... | collective-permute-start | bytes 73736 | tf_op jit(solution)/shard_map/ppermute | solution.py:661
  38.4 18.1 %all-to-all-start.1 = ((bf16[64,16,128]{2,1,0:T(8,128)(2,1)}), bf16[64,16,128]{2,1,0:T(8,128)(2,1)S(1)}, u32[]{:S(2)}, u32[]{:S(2)}) async-start(bf16[64,16,128]{2,1,0:T(8,128)(2,1)} %chain.1), calls=%async_computation.1 | async-start | bytes 524288 | tf_op jit(solution)/shard_map/all_to_all | solution.py:611
  62.3 54.0 %all-to-all-start.2 = ((bf16[4,96,2048]{2,1,0:T(8,128)(2,1)}), bf16[4,96,2048]{2,1,0:T(8,128)(2,1)S(1)}, u32[]{:S(2)}, u32[]{:S(2)}) async-start(bf16[4,96,2048]{2,1,0:T(8,128)(2,1)} %bitcast.6), calls=%async_computation.2 | async-start | bytes 3145728 | tf_op jit(solution)/shard_map/all_to_all | solution.py:611
  66.8 43.2 %collective-permute-start = (bf16[2048,256]{1,0:T(8,128)(2,1)S(1)}, bf16[2048,256]{1,0:T(8,128)(2,1)S(1)}, u32[]{:S(2)}, u32[]{:S(2)}) collective-permute-start(bf16[2048,256]{1,0:T(8,128)(2,1)S(1)} %bitcast.30), channel_id=1, source_target_pairs={{0,1},{1,2},{2,3},{3,0},{4,5},{5,6},{6,7},{7,4},{8,9},{9,10},{10,1... | collective-permute-start | bytes 3145736 | tf_op jit(solution)/shard_map/ppermute | solution.py:607
  68.8 41.2 %collective-permute-start.1 = (bf16[2048,256]{1,0:T(8,128)(2,1)}, bf16[2048,256]{1,0:T(8,128)(2,1)S(1)}, u32[]{:S(2)}, u32[]{:S(2)}) collective-permute-start(bf16[2048,256]{1,0:T(8,128)(2,1)} %bitcast.31), channel_id=1, source_target_pairs={{0,3},{1,0},{2,1},{3,2},{4,7},{5,4},{6,5},{7,6},{8,11},{9,8},{10,9... | collective-permute-start | bytes 3145736 | tf_op jit(solution)/shard_map/ppermute | solution.py:607
  72.2 44.0 %copy-start.4 = (bf16[96,2048]{1,0:T(8,128)(2,1)S(1)}, bf16[96,2048]{1,0:T(8,128)(2,1)}, u32[]{:S(2)}) copy-start(bf16[96,2048]{1,0:T(8,128)(2,1)} %refs_1_.3) | copy-start | bytes 1179652
  72.3 44.0 %copy-start.10 = (f32[2048]{0:T(1024)S(1)}, f32[2048]{0:T(1024)}, u32[]{:S(2)}) copy-start(f32[2048]{0:T(1024)} %param.39) | copy-start | bytes 24580
  72.3 44.0 %copy-start.11 = (f32[2048]{0:T(1024)S(1)}, f32[2048]{0:T(1024)}, u32[]{:S(2)}) copy-start(f32[2048]{0:T(1024)} %param.40) | copy-start | bytes 24580
  118.8 98.4 %all-to-all-start.3 = ((bf16[64,80,128]{2,1,0:T(8,128)(2,1)}), bf16[64,80,128]{2,1,0:T(8,128)(2,1)S(1)}, u32[]{:S(2)}, u32[]{:S(2)}) async-start(bf16[64,80,128]{2,1,0:T(8,128)(2,1)} %bitcast.10), calls=%async_computation.3 | async-start | bytes 2621440 | tf_op jit(solution)/shard_map/all_to_all | solution.py:611
  125.3 90.5 %collective-permute-start.7 = (bf16[3840,256]{1,0:T(8,128)(2,1)}, bf16[3840,256]{1,0:T(8,128)(2,1)S(1)}, u32[]{:S(2)}, u32[]{:S(2)}) collective-permute-start(bf16[3840,256]{1,0:T(8,128)(2,1)} %get-tuple-element.52), channel_id=1, source_target_pairs={{0,1},{1,2},{2,3},{3,0},{4,5},{5,6},{6,7},{7,4},{8,9},{9,10},{10,1... | collective-permute-start | bytes 5898248 | tf_op jit(solution)/shard_map/ppermute | solution.py:607
  125.4 91.7 %collective-permute-start.8 = (bf16[3840,256]{1,0:T(8,128)(2,1)}, bf16[3840,256]{1,0:T(8,128)(2,1)}, u32[]{:S(2)}, u32[]{:S(2)}) collective-permute-start(bf16[3840,256]{1,0:T(8,128)(2,1)} %get-tuple-element.53), channel_id=1, source_target_pairs={{0,3},{1,0},{2,1},{3,2},{4,7},{5,4},{6,5},{7,6},{8,11},{9,8},{10,9... | collective-permute-start | bytes 5898248 | tf_op jit(solution)/shard_map/ppermute | solution.py:607
  128.6 65.5 %collective-permute-start.3 = (bf16[2048,256]{1,0:T(8,128)(2,1)S(1)}, bf16[2048,256]{1,0:T(8,128)(2,1)S(1)}, u32[]{:S(2)}, u32[]{:S(2)}) collective-permute-start(bf16[2048,256]{1,0:T(8,128)(2,1)S(1)} %bitcast.36), channel_id=1, source_target_pairs={{0,1},{1,2},{2,3},{3,0},{4,5},{5,6},{6,7},{7,4},{8,9},{9,10},{10,1... | collective-permute-start | bytes 3145736 | tf_op jit(solution)/shard_map/ppermute | solution.py:607
  128.6 65.5 %collective-permute-start.4 = (bf16[2048,256]{1,0:T(8,128)(2,1)S(1)}, bf16[2048,256]{1,0:T(8,128)(2,1)S(1)}, u32[]{:S(2)}, u32[]{:S(2)}) collective-permute-start(bf16[2048,256]{1,0:T(8,128)(2,1)S(1)} %bitcast.37), channel_id=1, source_target_pairs={{0,3},{1,0},{2,1},{3,2},{4,7},{5,4},{6,5},{7,6},{8,11},{9,8},{10,9... | collective-permute-start | bytes 3145736 | tf_op jit(solution)/shard_map/ppermute | solution.py:607
  198.4 17.4 %collective-permute-start.5 = (bf16[1280,256]{1,0:T(8,128)(2,1)}, bf16[1280,256]{1,0:T(8,128)(2,1)S(1)}, u32[]{:S(2)}, u32[]{:S(2)}) collective-permute-start(bf16[1280,256]{1,0:T(8,128)(2,1)} %get-tuple-element.50), channel_id=1, source_target_pairs={{0,1},{1,2},{2,3},{3,0},{4,5},{5,6},{6,7},{7,4},{8,9},{9,10},{10,1... | collective-permute-start | bytes 1966088 | tf_op jit(solution)/shard_map/ppermute | solution.py:607
  198.5 17.3 %collective-permute-start.6 = (bf16[1280,256]{1,0:T(8,128)(2,1)}, bf16[1280,256]{1,0:T(8,128)(2,1)S(1)}, u32[]{:S(2)}, u32[]{:S(2)}) collective-permute-start(bf16[1280,256]{1,0:T(8,128)(2,1)} %get-tuple-element.51), channel_id=1, source_target_pairs={{0,3},{1,0},{2,1},{3,2},{4,7},{5,4},{6,5},{7,6},{8,11},{9,8},{10,9... | collective-permute-start | bytes 1966088 | tf_op jit(solution)/shard_map/ppermute | solution.py:607
  224.2 44.7 %copy-start.12 = (f32[2048]{0:T(1024)S(1)}, f32[2048]{0:T(1024)}, u32[]{:S(2)}) copy-start(f32[2048]{0:T(1024)} %param.46) | copy-start | bytes 24580
  224.3 44.7 %copy-start.13 = (f32[2048]{0:T(1024)S(1)}, f32[2048]{0:T(1024)}, u32[]{:S(2)}) copy-start(f32[2048]{0:T(1024)} %param.47) | copy-start | bytes 24580
  224.3 44.6 %copy-start.15 = (f32[96,2]{0,1:T(2,128)S(1)}, f32[96,2]{0,1:T(2,128)}, u32[]{:S(2)}) copy-start(f32[96,2]{0,1:T(2,128)} %param.42) | copy-start | bytes 2308
  (16 other events, 36.2 us)
